TPU v7x, 256 devices: a whole 4x4x8 slice. The times are simulated.
256 devices in a mesh: sp: 64 (over z, y, core), tp: 4 (over x).
Axes of the slice: x: 4, y: 4, z: 8, core: 2. Of those that a mesh axis runs over, the one named last changes fastest.
Arguments:
- stream: bfloat16 [16384, 2048], P(('sp', 'tp')), may hold values from -6 to 6
- query_one: bfloat16 [16384, 512], P('sp', 'tp'), may hold values from -280 to 280
- key_one: bfloat16 [16384, 512], P('sp', 'tp'), may hold values from -6 to 6
- query_two: bfloat16 [16384, 512], P('sp', 'tp'), may hold values from -280 to 280
- key_two: bfloat16 [16384, 512], P('sp', 'tp'), may hold values from -6 to 6
- values: bfloat16 [16384, 1024], P('sp', 'tp'), may hold values from -6 to 6
- lambdas: float32 [8], P('tp'), may hold values from 0.3 to 0.8
- head_gain: float32 [128], replicated, may hold values from 0.1 to 1.9
- out_weight: bfloat16 [1024, 2048], replicated, may hold values from -0.1875 to 0.1875
- norm_gain: float32 [2048], replicated, may hold values from 0.1 to 1.9
- gate_weight: bfloat16 [2048, 2816], P('sp', 'tp'), may hold values from -0.125 to 0.125
- up_weight: bfloat16 [2048, 2816], P('sp', 'tp'), may hold values from -0.125 to 0.125
- down_weight: bfloat16 [2816, 2048], P('tp', 'sp'), may hold values from -0.3125 to 0.3125
Outputs:
- result: bfloat16 [16384, 2048], P(('sp', 'tp'))
All inputs are finite; a program needn't handle non-finite values.
Results may differ from a plain program's by a relative error of at most 0.014.
Values may be sent and summed in bfloat16 or wider, within the bound.
A program may use at most 128 MiB of HBM per device.

v0:
```python
import math

import jax
import jax.numpy as jnp
from jax import lax
from jax.sharding import PartitionSpec as P

HEAD_DIM = 64


ALPHA = 1.4142135623730951
EPSILON = 1e-05


def sent_together(arrays, axis, dim, along):
    widths = [a.shape[along] for a in arrays]
    both = jnp.concatenate(arrays, axis=along)
    result = lax.all_gather(both, axis, axis=dim, tiled=True)
    return tuple(jnp.split(result, [sum(widths[:k]) for k in range(1, len(widths))], axis=along))


def sent_to_all(shard, axis):
    copies = jnp.broadcast_to(shard, (lax.axis_size(axis), *shard.shape))
    return lax.all_to_all(copies, axis, split_axis=0, concat_axis=0, tiled=True)


def in_order(blocks, dim):
    shape = list(blocks.shape[1:])
    shape[dim] *= blocks.shape[0]
    return jnp.moveaxis(blocks, 0, dim).reshape(shape)


def gathered_copies(shard, axis, dim):
    blocks = sent_to_all(shard, axis)
    return in_order(blocks, dim)


def turned_gather(arrays, axis, dims):
    turned = [jnp.moveaxis(a, dim, 0) for a, dim in zip(arrays, dims)]
    both = jnp.concatenate([t.reshape(len(t), -1) for t in turned], axis=1)
    result, at, gathered = (lax.all_gather(both, axis, axis=0, tiled=True), 0, [])
    for t, dim in zip(turned, dims):
        piece = result[:, at : at + t[0].size].reshape(-1, *t.shape[1:])
        gathered.append(jnp.moveaxis(piece, 0, dim))
        at += t[0].size
    return tuple(gathered)


def cut_along(shard, dim, count):
    before, after = (shard.shape[:dim], shard.shape[dim + 1 :])
    return jnp.moveaxis(shard.reshape(*before, count, -1, *after), dim, 0)


def sum_at_owner(shard, axis, dim):
    count = lax.axis_size(axis)
    blocks = lax.all_to_all(cut_along(shard, dim, count), axis, 0, 0, tiled=True)
    return jnp.sum(blocks.astype(jnp.float32), axis=0)


def update(carried, queries, keys, value_rows, factor):
    maxima, totals, weighted = carried
    scores = jnp.einsum("qhd,khd->hqk", queries, keys, preferred_element_type=jnp.float32) * factor
    new_maxima = jnp.maximum(maxima, jnp.max(scores, axis=-1))
    rescale = jnp.exp(maxima - new_maxima)
    weights = jnp.exp(scores - new_maxima[:, :, None])
    totals = totals * rescale + jnp.sum(weights, axis=-1)
    weighted = weighted * jnp.transpose(rescale)[:, :, None] + jnp.einsum(
        "hqk,khe->qhe", weights.astype(jnp.bfloat16), value_rows, preferred_element_type=jnp.float32
    )
    return (new_maxima, totals, weighted)


def finish(carried):
    maxima, totals, weighted = carried
    return weighted / jnp.transpose(totals)[:, :, None]


def layer_normed(heads_rows, residual_rows, out_weight, norm_gain):
    branch = jnp.dot(heads_rows, out_weight, preferred_element_type=jnp.float32)
    mixed_in = ALPHA * residual_rows.astype(jnp.float32) + branch
    row_mean = jnp.mean(mixed_in, axis=-1, keepdims=True)
    centered = mixed_in - row_mean
    row_var = jnp.mean(centered * centered, axis=-1, keepdims=True)
    return (centered * lax.rsqrt(row_var + EPSILON) * norm_gain).astype(jnp.bfloat16)


def sectioned_length(shard_len, group):
    return shard_len * math.gcd(128 // shard_len, group)


def sectioned_absorb(state, pieces, offset, along, block_len, work):
    running, sectioning, filled = state
    length = pieces[0].shape[along]
    sectioning = tuple((piece for piece in pieces))
    block_starts = jnp.arange(filled.shape[0], dtype=jnp.int32) * block_len
    covered = jnp.minimum(offset + length, block_starts + block_len) - jnp.maximum(
        offset, block_starts
    )
    covered = jnp.clip(covered, 0, block_len)
    before = filled
    filled = covered
    completed = (filled == block_len) & (before < block_len)

    def visit_block(block_index, totals):
        begin_at = block_index * block_len

        def compute(inner):
            slices = tuple(
                (
                    lax.dynamic_slice_in_dim(holder, begin_at, block_len, along)
                    for holder in sectioning
                )
            )
            return work(inner, slices, begin_at)

        def unchanged(inner):
            return inner

        return lax.cond(completed[block_index], compute, unchanged, totals)

    running = lax.fori_loop(0, filled.shape[0], visit_block, running)
    return (running, sectioning, filled)


def on_device(
    stream,
    query_one,
    key_one,
    query_two,
    key_two,
    values,
    lambdas,
    head_gain,
    out_weight,
    norm_gain,
    gate_weight,
    up_weight,
    down_weight,
):
    local_heads = lambdas.shape[0]
    head_width = query_one.shape[1] // local_heads
    value_width = values.shape[1] // local_heads
    tokens = query_one.shape[0]
    group = lax.axis_size("sp")
    factor = HEAD_DIM ** (-0.5)
    gate_full, up_full = sent_together((gate_weight, up_weight), "sp", 0, 1)
    queries_first = query_one.reshape(tokens, local_heads, head_width)
    queries_second = query_two.reshape(tokens, local_heads, head_width)
    initial = (
        jnp.full((local_heads, tokens), -1e30, jnp.float32),
        jnp.zeros((local_heads, tokens), jnp.float32),
        jnp.zeros((tokens, local_heads, value_width), jnp.float32),
    )
    first_keys, second_keys, value_rows = sent_together((key_one, key_two, values), "sp", 0, 1)
    length = first_keys.shape[0]
    block_len = length
    while block_len > 2048 and block_len % 2 == 0:
        block_len = block_len // 2
    first_keys = first_keys.reshape(length, local_heads, head_width)
    second_keys = second_keys.reshape(length, local_heads, head_width)
    value_rows = value_rows.reshape(length, local_heads, value_width)

    def advance(block_index, partial_value):
        begin_row = block_index * block_len
        keys_first = lax.dynamic_slice_in_dim(first_keys, begin_row, block_len, 0)
        keys_second = lax.dynamic_slice_in_dim(second_keys, begin_row, block_len, 0)
        block_values = lax.dynamic_slice_in_dim(value_rows, begin_row, block_len, 0)
        return (
            update(partial_value[0], queries_first, keys_first, block_values, factor),
            update(partial_value[1], queries_second, keys_second, block_values, factor),
        )

    first_state, second_state = lax.fori_loop(0, length // block_len, advance, (initial, initial))
    differ = finish(first_state) - lambdas[None, :, None] * finish(second_state)
    inverse_rms = lax.rsqrt(jnp.mean(differ * differ, axis=-1, keepdims=True) + EPSILON)
    attended = (
        (differ * inverse_rms * head_gain * 0.8)
        .astype(jnp.bfloat16)
        .reshape(tokens, local_heads * value_width)
    )
    by_rows = lax.all_to_all(attended, "tp", split_axis=0, concat_axis=1, tiled=True)
    own_normed = layer_normed(by_rows, stream, out_weight, norm_gain)
    normed_all = gathered_copies(own_normed, "tp", 0)
    row_count = normed_all.shape[0]
    gate_out = jnp.dot(normed_all, gate_full, preferred_element_type=jnp.float32)
    upward = jnp.dot(normed_all, up_full, preferred_element_type=jnp.float32)
    hidden = (jax.nn.silu(gate_out) * upward).astype(jnp.bfloat16)
    column_width = down_weight.shape[1]
    columns_block = sectioned_length(column_width, group)

    def project_block(outputs, slices, begin_at):
        product = jnp.dot(hidden, slices[0], preferred_element_type=jnp.float32)
        return lax.dynamic_update_slice_in_dim(outputs, product, begin_at, 1)

    project_start = (
        jnp.zeros((row_count, column_width * group), jnp.float32),
        (jnp.zeros((down_weight.shape[0], column_width * group), jnp.bfloat16),),
        jnp.zeros((column_width * group // columns_block,), jnp.int32),
    )
    project_state = sectioned_absorb(
        project_start,
        turned_gather((down_weight,), "sp", (1,)),
        jnp.int32(0),
        1,
        columns_block,
        project_block,
    )
    partial_terms = project_state[0]
    mixer_out = sum_at_owner(partial_terms.astype(jnp.bfloat16), "tp", 0)
    return (ALPHA * own_normed.astype(jnp.float32) + 0.5 * mixer_out).astype(jnp.bfloat16)


def solution(mesh):
    return jax.shard_map(
        on_device,
        mesh=mesh,
        in_specs=(
            P(("sp", "tp"), None),
            P("sp", "tp"),
            P("sp", "tp"),
            P("sp", "tp"),
            P("sp", "tp"),
            P("sp", "tp"),
            P("tp"),
            P(),
            P(),
            P(),
            P("sp", "tp"),
            P("sp", "tp"),
            P("tp", "sp"),
        ),
        out_specs=P(("sp", "tp"), None),
        check_vma=False,
    )
```

profile of v0, /device:TPU:1, one launch (start us, length us, event | category | flops | bytes accessed | tf_op | source)
XLA Modules:
  0.0 355.6 jit_solution(1471579178897296748)
XLA Ops:
  12.5 101.1 %all-gather.4.cloned.1.call-done = bf16[16384,512]{1,0:T(8,128)(2,1)} async-done(((bf16[256,512]{1,0:T(8,128)(2,1)}), bf16[16384,512]{1,0:T(8,128)(2,1)}) %all-gather.4.cloned.1.call-update) | async-done | bytes 16777232 | tf_op jit(solution)/shard_map/all_gather | solution.py:18
  113.6 5.8 %fusion.59 = (bf16[16384,128]{1,0:T(8,128)(2,1)}, bf16[16384,128]{1,0:T(8,128)(2,1)}) fusion(bf16[16384,512]{1,0:T(8,128)(2,1)} %all-gather.4.cloned.1.call-done), kind=kLoop, calls=%fused_computation.70 | loop fusion | bytes 16777216 | tf_op jit(solution)/shard_map/split | solution.py:19
  119.4 6.5 %copy.37 = bf16[16384,128]{0,1:T(8,128)(2,1)} copy(bf16[16384,128]{1,0:T(8,128)(2,1)} %get-tuple-element.437) | data formatting | bytes 8388608 | tf_op jit(solution)/shard_map/split | solution.py:19
  125.8 6.4 %copy.40 = bf16[16384,128]{0,1:T(8,128)(2,1)} copy(bf16[16384,128]{1,0:T(8,128)(2,1)} %get-tuple-element.436) | data formatting | bytes 8388608 | tf_op jit(solution)/shard_map/split | solution.py:19
  132.3 7.1 %split.21 = bf16[16384,256]{1,0:T(8,128)(2,1)} slice(bf16[16384,512]{1,0:T(8,128)(2,1)} %all-gather.4.cloned.1.call-done), slice={[0:16384], [256:512]} | slice | bytes 16777216 | tf_op jit(solution)/shard_map/split | solution.py:19
  139.4 11.9 %copy.39 = bf16[16384,256]{0,1:T(8,128)(2,1)} copy(bf16[16384,256]{1,0:T(8,128)(2,1)} %split.21) | data formatting | bytes 16777216 | tf_op jit(solution)/shard_map/split | solution.py:19
  151.2 103.1 %while.41 = (s32[]{:T(128)}, f32[2,256]{1,0:T(2,128)S(1)}, f32[2,256]{1,0:T(2,128)S(1)}, f32[256,2,128]{0,2,1:T(8,128)S(1)}, f32[2,256]{1,0:T(2,128)S(1)}, /*ind...) while((s32[]{:T(128)}, f32[2,256]{1,0:T(2,128)S(1)}, ...), condition=%wide.region_5.0_spmd.clone, body=%wide.region_0.0_spmd.clone.sunk | while | flops 822482944 | bytes 46334200 | solution.py:173
  151.3 3.8 %bitcast_reduce_fusion.5 = (f32[2,256]{1,0:T(2,128)S(1)}, f32[2,2048,256]{2,1,0:T(8,128)}) fusion(bf16[256,2,64]{0,2,1:T(8,128)(2,1)S(1)} %get-tuple-element.607, bf16[16384,2,64]{0,2,1:T(8,128)(2,1)} %get-tuple-element.606, s32[]{:T(128)S(6)} %select_n.21), kind=kOutput, calls=%fused_computation.5.clone.1 | convolution fusion | flops 136314368 | bytes 4786180 | tf_op jit(solution)/shard_map/while/body/eval_jaxpr/qhd,khd->hqk/dot_general | solution.py:62
  155.1 3.4 fusion.93
  164.1 3.8 %bitcast_reduce_fusion.5 = (f32[2,256]{1,0:T(2,128)S(1)}, f32[2,2048,256]{2,1,0:T(8,128)}) fusion(bf16[256,2,64]{0,2,1:T(8,128)(2,1)S(1)} %get-tuple-element.607, bf16[16384,2,64]{0,2,1:T(8,128)(2,1)} %get-tuple-element.606, s32[]{:T(128)S(6)} %select_n.21), kind=kOutput, calls=%fused_computation.5.clone.1 | convolution fusion | flops 136314368 | bytes 4786180 | tf_op jit(solution)/shard_map/while/body/eval_jaxpr/qhd,khd->hqk/dot_general | solution.py:62
  167.9 3.4 fusion.93
  177.0 3.8 %bitcast_reduce_fusion.5 = (f32[2,256]{1,0:T(2,128)S(1)}, f32[2,2048,256]{2,1,0:T(8,128)}) fusion(bf16[256,2,64]{0,2,1:T(8,128)(2,1)S(1)} %get-tuple-element.607, bf16[16384,2,64]{0,2,1:T(8,128)(2,1)} %get-tuple-element.606, s32[]{:T(128)S(6)} %select_n.21), kind=kOutput, calls=%fused_computation.5.clone.1 | convolution fusion | flops 136314368 | bytes 4786180 | tf_op jit(solution)/shard_map/while/body/eval_jaxpr/qhd,khd->hqk/dot_general | solution.py:62
  180.8 3.4 fusion.93
  189.9 3.8 %bitcast_reduce_fusion.5 = (f32[2,256]{1,0:T(2,128)S(1)}, f32[2,2048,256]{2,1,0:T(8,128)}) fusion(bf16[256,2,64]{0,2,1:T(8,128)(2,1)S(1)} %get-tuple-element.607, bf16[16384,2,64]{0,2,1:T(8,128)(2,1)} %get-tuple-element.606, s32[]{:T(128)S(6)} %select_n.21), kind=kOutput, calls=%fused_computation.5.clone.1 | convolution fusion | flops 136314368 | bytes 4786180 | tf_op jit(solution)/shard_map/while/body/eval_jaxpr/qhd,khd->hqk/dot_general | solution.py:62
  193.7 3.4 fusion.93
  202.8 3.8 %bitcast_reduce_fusion.5 = (f32[2,256]{1,0:T(2,128)S(1)}, f32[2,2048,256]{2,1,0:T(8,128)}) fusion(bf16[256,2,64]{0,2,1:T(8,128)(2,1)S(1)} %get-tuple-element.607, bf16[16384,2,64]{0,2,1:T(8,128)(2,1)} %get-tuple-element.606, s32[]{:T(128)S(6)} %select_n.21), kind=kOutput, calls=%fused_computation.5.clone.1 | convolution fusion | flops 136314368 | bytes 4786180 | tf_op jit(solution)/shard_map/while/body/eval_jaxpr/qhd,khd->hqk/dot_general | solution.py:62
  206.5 3.4 fusion.93
  215.6 3.8 %bitcast_reduce_fusion.5 = (f32[2,256]{1,0:T(2,128)S(1)}, f32[2,2048,256]{2,1,0:T(8,128)}) fusion(bf16[256,2,64]{0,2,1:T(8,128)(2,1)S(1)} %get-tuple-element.607, bf16[16384,2,64]{0,2,1:T(8,128)(2,1)} %get-tuple-element.606, s32[]{:T(128)S(6)} %select_n.21), kind=kOutput, calls=%fused_computation.5.clone.1 | convolution fusion | flops 136314368 | bytes 4786180 | tf_op jit(solution)/shard_map/while/body/eval_jaxpr/qhd,khd->hqk/dot_general | solution.py:62
  219.4 3.4 fusion.93
  228.5 3.8 %bitcast_reduce_fusion.5 = (f32[2,256]{1,0:T(2,128)S(1)}, f32[2,2048,256]{2,1,0:T(8,128)}) fusion(bf16[256,2,64]{0,2,1:T(8,128)(2,1)S(1)} %get-tuple-element.607, bf16[16384,2,64]{0,2,1:T(8,128)(2,1)} %get-tuple-element.606, s32[]{:T(128)S(6)} %select_n.21), kind=kOutput, calls=%fused_computation.5.clone.1 | convolution fusion | flops 136314368 | bytes 4786180 | tf_op jit(solution)/shard_map/while/body/eval_jaxpr/qhd,khd->hqk/dot_general | solution.py:62
  232.2 3.4 fusion.93
  241.3 3.8 %bitcast_reduce_fusion.5 = (f32[2,256]{1,0:T(2,128)S(1)}, f32[2,2048,256]{2,1,0:T(8,128)}) fusion(bf16[256,2,64]{0,2,1:T(8,128)(2,1)S(1)} %get-tuple-element.607, bf16[16384,2,64]{0,2,1:T(8,128)(2,1)} %get-tuple-element.606, s32[]{:T(128)S(6)} %select_n.21), kind=kOutput, calls=%fused_computation.5.clone.1 | convolution fusion | flops 136314368 | bytes 4786180 | tf_op jit(solution)/shard_map/while/body/eval_jaxpr/qhd,khd->hqk/dot_general | solution.py:62
  245.1 3.6 %fusion.93 = f32[256,2,128]{0,2,1:T(8,128)S(1)} fusion(f32[2,2048,256]{2,1,0:T(8,128)} %get-tuple-element.556, f32[2,256]{1,0:T(2,128)S(1)} %get-tuple-element.600, bf16[16384,2,128]{0,2,1:T(8,128)(2,1)} %get-tuple-element.605, s32[]{:T(128)S(6)} %select_n.21, f32[256,2,128]{0,2,1:T(8,128)S(1)} %get-tuple-element.586, ...), kind=kOutput, calls=%fused_computation.23.clone.1 | convolution fusion | flops 271777792 | bytes 5771269 | tf_op jit(solution)/shard_map/while/body/eval_jaxpr/hqk,khe->qhe/dot_general | solution.py:67
  254.8 8.6 %all_to_all.29 = bf16[4,64,256]{2,1,0:T(8,128)(2,1)S(1)} all-to-all(bf16[4,64,256]{2,1,0:T(8,128)(2,1)S(1)} %all_to_all.20), channel_id=1, replica_groups=mesh['sp'=64,'tp'=4] {'tp'}, dimensions={0} | all-to-all | bytes 262144 | tf_op jit(solution)/shard_map/all_to_all | solution.py:181
  263.5 3.2 fusion.60
  268.3 3.7 %all-to-all-start.1 = ((bf16[4,64,2048]{2,1,0:T(8,128)(2,1)}), bf16[4,64,2048]{2,1,0:T(8,128)(2,1)S(1)}, u32[]{:S(2)}, u32[]{:S(2)}) async-start(bf16[4,64,2048]{2,1,0:T(8,128)(2,1)} %broadcast_in_dim.39), calls=%async_computation.1 | async-start | bytes 2097152 | tf_op jit(solution)/shard_map/all_to_all | solution.py:24
  272.0 4.7 %copy.44 = bf16[704,2048]{1,0:T(8,128)(2,1)} copy(bf16[704,2048]{0,1:T(8,128)(2,1)} %bitcast.96) | data formatting | bytes 5767168 | tf_op jit(solution)/shard_map/while | solution.py:121
  276.8 8.7 %all-to-all-done.1 = bf16[4,64,2048]{2,1,0:T(8,128)(2,1)S(1)} async-done(((bf16[4,64,2048]{2,1,0:T(8,128)(2,1)}), bf16[4,64,2048]{2,1,0:T(8,128)(2,1)S(1)}, u32[]{:S(2)}, u32[]{:S(2)}) %all-to-all-start.1) | async-done | bytes 1048608 | tf_op jit(solution)/shard_map/all_to_all | solution.py:24
  285.5 3.3 fusion.49
  289.0 2.7 fusion.54
  292.0 40.1 %while.40 = (s32[]{:T(128)}, bf16[256,2048]{0,1:T(8,128)(2,1)S(1)}, pred[16]{0:T(512)(128)(4,1)S(1)}, bf16[704,2048]{1,0:T(8,128)(2,1)}, bf16[256,704]{1,0:T(8,128)(2,1)S(1)}, /*index=5*/s32[]{:T(128)}) while((s32[]{:T(128)}, bf16[256,2048]{0,1:T(8,128)(2,1)S(1)}, pred[16]{0:T(512)(128)(4,1)S(1)}, bf16[704,2048]{1,0:T(8,128)(2,1)}, ...), condition=%wide.region_12.13_spmd, body=%wide.region_9.12_spmd.sunk | while | flops 46137352 | bytes 705702 | solution.py:121
  332.7 15.3 %all_to_all.30 = bf16[4,64,2048]{2,1,0:T(8,128)(2,1)S(1)} all-to-all(bf16[4,64,2048]{2,1,0:T(8,128)(2,1)S(1)} %bitcast.95), channel_id=1, replica_groups=mesh['sp'=64,'tp'=4] {'tp'}, dimensions={0} | all-to-all | bytes 2097152 | tf_op jit(solution)/shard_map/all_to_all | solution.py:56
  (181 shorter events, 103.6 us)
Async XLA Ops:
  6.5 107.1 %all-gather.4.cloned.1.call-start = ((), (), s32[]{:S(2)}) async-start(), calls=%async_computation.3 | async-start | bytes 17039360 | tf_op jit(solution)/shard_map/all_gather | solution.py:18
  8.2 263.8 %all-gather.6.cloned.1.call-start = ((), (), s32[]{:S(2)}) async-start(), calls=%async_computation.4 | async-start | bytes 3194880 | tf_op jit(solution)/shard_map/all_gather | solution.py:41
  9.0 267.8 %all-gather.8.cloned.1.call-start = ((), (), s32[]{:S(2)}) async-start(), calls=%async_computation.5 | async-start | bytes 5857280 | tf_op jit(solution)/shard_map/all_gather | solution.py:18
  151.2 103.1 %copy-start.4 = (f32[2]{0:T(128)S(1)}, f32[2]{0:T(128)}, u32[]{:S(2)}) copy-start(f32[2]{0:T(128)} %param.25) | copy-start | bytes 28
  151.2 103.3 %copy-start.3 = (f32[128]{0:T(128)S(1)}, f32[128]{0:T(128)}, u32[]{:S(2)}) copy-start(f32[128]{0:T(128)} %param.26) | copy-start | bytes 1540
  151.2 112.3 %copy-start.1 = (bf16[64,2048]{1,0:T(8,128)(2,1)S(1)}, bf16[64,2048]{1,0:T(8,128)(2,1)}, u32[]{:S(2)}) copy-start(bf16[64,2048]{1,0:T(8,128)(2,1)} %param.19) | copy-start | bytes 786436
  160.3 3.0 copy-start
  173.2 3.1 copy-start
  186.1 3.0 copy-start
  198.9 3.0 copy-start
  211.8 3.0 copy-start
  224.7 3.0 copy-start
  237.5 3.0 copy-start
  250.6 3.0 copy-start
  254.4 12.7 %copy-start.2 = (f32[2048]{0:T(1024)S(1)}, f32[2048]{0:T(1024)}, u32[]{:S(2)}) copy-start(f32[2048]{0:T(1024)} %param.28) | copy-start | bytes 24580
  268.3 17.2 %all-to-all-start.1 = ((bf16[4,64,2048]{2,1,0:T(8,128)(2,1)}), bf16[4,64,2048]{2,1,0:T(8,128)(2,1)S(1)}, u32[]{:S(2)}, u32[]{:S(2)}) async-start(bf16[4,64,2048]{2,1,0:T(8,128)(2,1)} %broadcast_in_dim.39), calls=%async_computation.1 | async-start | bytes 2097152 | tf_op jit(solution)/shard_map/all_to_all | solution.py:24
  285.5 3.6 %copy-start.5 = (bf16[2048,1408]{1,0:T(8,128)(2,1)S(1)}, bf16[2048,1408]{1,0:T(8,128)(2,1)}, u32[]{:S(2)}) copy-start(bf16[2048,1408]{1,0:T(8,128)(2,1)} %all-gather.8.cloned.1.call-done) | copy-start | bytes 17301508
Sparse Core Ops, SparseCore 0:
  10.1 103.4 all-gather.3
  116.4 75.0 all-gather.5
  194.2 77.5 all-gather.7
where the time goes:
time: 359 us; the launch traced here: 356 us
  matrix products  120 us (33%)
  waiting for transfers between devices  110 us (31%)
  local copies, waits for them, and re-layouts  56.2 us (16%)
  blocking collectives  23.9 us (7%)
  other arithmetic  16.4 us (5%)
  between operations  13.3 us (4%)
  loops' own time  11.8 us (3%)
  starting transfers between devices  3.78 us (1%)
    all_gather x2, waiting for transfers between devices, sent_together(): result = lax.all_gather(both, axis, axis=dim, tiled=True)  101 us
    dot_general x16, matrix products, update(): jnp.einsum('hqk,khe->qhe', weights.astype(jnp.bfloat16), value_rows, pref...  46.2 us
    dot_general x16, matrix products, update(): jnp.einsum('qhd,khd->hqk', queries, keys, preferred_element_type=jnp.floa...  44.6 us
    split x5, local copies, waits for them, and re-layouts, sent_together(): jnp.split(result, [sum(widths[:k]) for k in range(1, len(widths))], axis=...  37.6 us
    dot_general x16, matrix products, project_block(): product = jnp.dot(hidden, slices[0], preferred_element_type=jnp.float32)  19.5 us
    all_to_all x1, blocking collectives, sum_at_owner(): lax.all_to_all(cut_along(shard, dim, count), axis, 0, 0, tiled=True)  15.3 us
    reduce_sum x16, other arithmetic, update(): totals = totals * rescale + jnp.sum(weights, axis=-1)  11.2 us
    another operation x1, loops' own time, sectioned_absorb(): running = lax.fori_loop(0, filled.shape[0], visit_block, running)  10.7 us
  transfers between devices with their start and end apart: 4, of which 2 were waited for; matrix products, arithmetic and copies ran while one was open for 43% of the time, Pallas kernels for 0%

commit v1 on v0

v1 whole, which is shorter than its diff:
```python
import functools
import math

import jax
import jax.numpy as jnp
from jax import lax
from jax.experimental import pallas as pl
from jax.experimental.pallas import tpu as pltpu
from jax.sharding import PartitionSpec as P

MESH = pl.DeviceIdType.MESH
F32 = jnp.float32
BF16 = jnp.bfloat16
ALPHA = 1.4142135623730951
EPSILON = 1e-05
SCALE = math.log2(math.e) / 8.0
NB = 4
REL = (2, 1, 3, 0)
Z_OF_SLOT = (0, -1, 1, -2, 2, -3, 3, 4)


class Messages:
    def __init__(self):
        self.index = {}

    def of(self, name):
        return self.index.setdefault(name, len(self.index))


def message_names():
    names = [("q", p) for p in range(3)]
    for a in "kv":
        names += [(a, s) for s in range(1, 8)] + [(a + "d", s) for s in range(8)]
    names += [("t",)] + [("wz", s) for s in range(1, 7)] + [("wz7a",), ("wz7b",)]
    for kind in ("wxl", "wxr", "wxa", "wxb", "wd0", "wd1", "wd2", "wd3"):
        names += [(kind, i) for i in range(8)]
    names += [("s", j) for j in range(1, 4)]
    names += [("o", p) for p in range(3)] + [("st", p) for p in range(3)]
    names += [("a", dy, dx) for dy in range(4) for dx in range(4) if dy or dx]
    names += [("p", h, j) for h in range(2) for j in range(1, 4)]
    return names


NAMES = message_names()
INDEX = {name: i for i, name in enumerate(NAMES)}


def kernel(
    q_ref, k_ref, v_ref, w_ref, s_ref, lam_ref, hg_ref, ng_ref, wo_ref,
    out_ref,
    q_all, k_all, v_all, acc, m_st, l_st, sb0, sb1, w_all, s_all, wo_v,
    o_out, st_out, o_in, st_in, att_own, att, branch, normed, hidden, part, part_in,
    send_sems, recv_sems, local_sems,
):
    sp = lax.axis_index("sp")
    x = lax.axis_index("tp")
    z = sp // 8
    y = lax.rem(sp, 8) // 2
    c = lax.rem(sp, 2)

    def mod(a, n):
        return lax.rem(a + 2 * n, n)

    def at(dz=0, dy=0, dc=0, dx=0):
        return {
            "sp": mod(z + dz, 8) * 8 + mod(y + dy, 4) * 2 + mod(c + dc, 2),
            "tp": mod(x + dx, 4),
        }

    def block(dz=0, dx=0):
        return mod(z + dz, 8) * 8 + mod(x + dx, 4) * 2 + c

    def remote(name, src, dst, target):
        i = INDEX[name]
        return pltpu.make_async_remote_copy(
            src_ref=src, dst_ref=dst, send_sem=send_sems.at[i], recv_sem=recv_sems.at[i],
            device_id=target, device_id_type=MESH,
        )

    def describe(name):
        kind = name[0]
        if kind == "q":
            p = name[1]
            return remote(name, q_ref, q_all.at[p], at(dy=REL[p]))
        if kind in ("k", "v"):
            s = name[1]
            buf, own = (k_all, k_ref) if kind == "k" else (v_all, v_ref)
            step = 1 if s in (1, 3, 5) else -1
            before = s - 2
            if s == 7:
                step, before = (1, 5) if kind == "k" else (-1, 6)
            src = own if s <= 2 else buf.at[2 * before]
            return remote(name, src, buf.at[2 * s], at(dz=step))
        if kind in ("kd", "vd"):
            s = name[1]
            buf, own = (k_all, k_ref) if kind == "kd" else (v_all, v_ref)
            return remote(name, own if s == 0 else buf.at[2 * s], buf.at[2 * s + 1], at(dc=1))
        if kind == "t":
            return remote(name, w_ref, w_all.at[z * 8 + y * 2 + c], {"sp": z * 8 + x * 2 + c, "tp": y})
        if kind == "wz":
            s = name[1]
            step = 1 if s in (1, 3, 5) else -1
            ref = w_all.at[block(dz=Z_OF_SLOT[s - 2] if s > 2 else 0)]
            return remote(name, ref, ref, at(dz=step))
        if kind == "wz7a":
            ref = w_all.at[block(dz=-3), 0:48]
            return remote(name, ref, ref, at(dz=1))
        if kind == "wz7b":
            ref = w_all.at[block(dz=3), 48:96]
            return remote(name, ref, ref, at(dz=-1))
        if kind in ("wxl", "wxr"):
            ref = w_all.at[block(dz=Z_OF_SLOT[name[1]])]
            return remote(name, ref, ref, at(dx=1 if kind == "wxl" else -1))
        if kind == "wxa":
            ref = w_all.at[block(dz=Z_OF_SLOT[name[1]], dx=-1), 0:48]
            return remote(name, ref, ref, at(dx=1))
        if kind == "wxb":
            ref = w_all.at[block(dz=Z_OF_SLOT[name[1]], dx=1), 48:96]
            return remote(name, ref, ref, at(dx=-1))
        if kind[:2] == "wd":
            ref = w_all.at[block(dz=Z_OF_SLOT[name[1]], dx=(0, -1, 1, 2)[int(kind[2])])]
            return remote(name, ref, ref, at(dc=1))
        if kind == "s":
            return remote(name, s_ref, s_all.at[name[1]], at(dy=name[1]))
        if kind == "o":
            p = name[1]
            return remote(name, o_out.at[p], o_in.at[p], at(dy=-REL[p]))
        if kind == "st":
            p = name[1]
            return remote(name, st_out.at[p], st_in.at[p], at(dy=-REL[p]))
        if kind == "a":
            dy, dx = name[1:]
            rows = pl.multiple_of(mod(x + dx, 4) * 64, 64)
            return remote(
                name, att_own.at[pl.ds(rows, 64)], att.at[x, dy * 64:(dy + 1) * 64], at(dy=dy, dx=dx)
            )
        if kind == "p":
            h, j = name[1:]
            return remote(name, part.at[h, j], part_in.at[h, j], at(dy=-j))
        raise KeyError(kind)

    def start(*names):
        for name in names:
            describe(name).start()

    def arrive(*names):
        for name in names:
            describe(name).wait_recv()

    barrier = pltpu.get_barrier_semaphore()
    partners = [at(dz=1), at(dz=-1), at(dc=1)]
    partners += [at(dy=dy, dx=dx) for dy in range(4) for dx in range(4) if dy or dx]
    for partner in partners:
        pl.semaphore_signal(barrier, inc=1, device_id=partner, device_id_type=MESH)
    wo_copy = pltpu.make_async_copy(wo_ref, wo_v, local_sems.at[0])
    wo_copy.start()
    q_all[3] = q_ref[...]
    k_all[0] = k_ref[...]
    v_all[0] = v_ref[...]
    s_all[0] = s_ref[...]
    m_st[...] = jnp.full_like(m_st, -1e30)
    l_st[...] = jnp.zeros_like(l_st)
    acc[...] = jnp.zeros_like(acc)
    pl.semaphore_wait(barrier, len(partners))

    own_w = pltpu.make_async_copy(w_ref, w_all.at[z * 8 + y * 2 + c], local_sems.at[1])
    stays = x == y
    start(("q", 0), ("k", 1), ("k", 2), ("kd", 0), ("v", 1), ("v", 2), ("vd", 0), ("q", 1), ("q", 2))

    @pl.when(stays)
    def _():
        own_w.start()

    @pl.when(jnp.logical_not(stays))
    def _():
        start(("t",))

    @pl.when(stays)
    def _():
        own_w.wait()

    @pl.when(jnp.logical_not(stays))
    def _():
        arrive(("t",))

    start(("wxl", 0), ("wxr", 0), ("wd0", 0))
    arrive(("q", 0), ("kd", 0), ("vd", 0), ("k", 1))
    start(("k", 3), ("kd", 1))
    arrive(("k", 2))
    start(("k", 4), ("kd", 2))
    arrive(("v", 1))
    start(("v", 3), ("vd", 1))
    arrive(("v", 2))
    start(("v", 4), ("vd", 2))
    start(("wz", 1), ("wz", 2))
    arrive(("kd", 1), ("vd", 1))

    def w_across(i):
        def act():
            start(("wxl", i), ("wxr", i), ("wd0", i))
        return act

    def w_on(i):
        def act():
            arrive(("wxl", i), ("wxr", i))
            start(("wxa", i), ("wxb", i), ("wd1", i), ("wd2", i))
        return act

    def w_last(i):
        def act():
            arrive(("wxa", i), ("wxb", i))
            start(("wd3", i))
        return act

    def ring_on(s):
        def act():
            for a in "kv":
                arrive((a, s), (a, s + 1))
                if s < 5:
                    start((a, s + 2), (a, s + 3))
                else:
                    start((a, 7))
                start((a + "d", s), (a + "d", s + 1))
        return act

    def ring_end():
        arrive(("k", 7), ("v", 7))
        start(("kd", 7), ("vd", 7))

    def copies(*slots):
        def act():
            for s in slots:
                arrive(("kd", s), ("vd", s))
        return act

    def w_ring(s):
        def act():
            arrive(("wz", s), ("wz", s + 1))
            if s < 5:
                start(("wz", s + 2), ("wz", s + 3))
            else:
                start(("wz7a",), ("wz7b",))
        return act

    def w_ring_end():
        arrive(("wz7a",), ("wz7b",))

    def finalize(p):
        def act():
            for hm in range(4):
                unit = p * 4 + hm
                total = jnp.sum(l_st[unit], axis=0, keepdims=True)
                o_out[p, hm * 128:(hm + 1) * 128, :] = (acc[unit] * (1.0 / total)).astype(BF16)
                st_out[p, hm:hm + 1, :] = m_st[unit, 0:1, :]
                st_out[p, 4 + hm:5 + hm, :] = total
            start(("o", p), ("st", p))
        return act

    events = {
        0: [lambda: arrive(("q", 1))],
        1: [lambda: arrive(("q", 2)), lambda: start(("s", 1), ("s", 3), ("s", 2))],
        2: [w_on(0)],
        3: [ring_on(3), copies(2, 3)],
        4: [w_ring(1), w_across(1), w_across(2), w_last(0)],
        7: [ring_on(5), copies(4, 5), w_on(1), w_on(2)],
        8: [w_ring(3), w_across(3), w_across(4)],
        10: [w_last(1), w_last(2)],
        11: [ring_end, copies(6, 7), w_on(3), w_on(4)],
        12: [w_ring(5), w_across(5), w_across(6)],
        13: [finalize(0), w_last(3), w_last(4)],
        14: [finalize(1)],
        15: [finalize(2), w_on(5), w_on(6)],
    }

    def scores(s_buf, qi, hm, first):
        m, h = hm // 2, hm % 2
        q = q_all[qi, :, m * 128:(m + 1) * 128]
        lane = lax.broadcasted_iota(jnp.int32, q.shape, 1)
        q = jnp.where((lane >= 64) if h else (lane < 64), q, jnp.zeros_like(q))
        peak = None
        for b in range(NB):
            s = lax.dot_general(
                k_all[first + b, :, m * 128:(m + 1) * 128], q, (((1,), (1,)), ((), ())),
                preferred_element_type=F32,
            )
            s_buf[b * 256:(b + 1) * 256, :] = s
            r = jnp.max(s.reshape(32, 8, 256), axis=0)
            peak = r if peak is None else jnp.maximum(peak, r)
        return peak

    def absorb(s_buf, unit, hm, first, peak):
        h = hm % 2
        m_old = m_st[unit]
        m_new = jnp.maximum(m_old, jnp.max(peak, axis=0, keepdims=True) * SCALE)
        rescale = jnp.exp2(m_old - m_new)
        m_st[unit] = m_new
        total, out = None, None
        for b in range(NB):
            s = s_buf[b * 256:(b + 1) * 256, :].reshape(32, 8, 256)
            weights = jnp.exp2(s * SCALE - m_new[None])
            t = jnp.sum(weights, axis=0)
            total = t if total is None else total + t
            o = jnp.dot(
                v_all[first + b, h * 128:(h + 1) * 128, :], weights.reshape(256, 256).astype(BF16),
                preferred_element_type=F32,
            )
            out = o if out is None else out + o
        l_st[unit] = l_st[unit] * rescale + total
        acc[unit] = (acc[unit].reshape(16, 8, 256) * rescale[None] + out.reshape(16, 8, 256)).reshape(128, 256)

    bufs = (sb0, sb1)
    first_peak = scores(bufs[0], 0, 0, 0)

    def body(t, peak):
        for when, actions in events.items():
            @pl.when(t == when)
            def _(actions=actions):
                for action in actions:
                    action()
        step, qi = t // 4, lax.rem(t, 4)
        later = jnp.minimum(t + 1, 15)
        for hm in range(4):
            if hm < 3:
                ahead = scores(bufs[(hm + 1) % 2], qi, hm + 1, step * NB)
            else:
                ahead = scores(bufs[0], lax.rem(later, 4), 0, (later // 4) * NB)
            absorb(bufs[hm % 2], qi * 4 + hm, hm, step * NB, peak)
            peak = ahead
        return peak

    lax.fori_loop(0, 16, body, first_peak)

    w_ring_end()
    w_across(7)()
    for p in range(3):
        arrive(("o", p), ("st", p))
    for h in range(2):
        maps = []
        for m in range(2):
            hm = m * 2 + h
            unit = 12 + hm
            peaks = [st_in[p, hm:hm + 1, :] for p in range(3)] + [m_st[unit, 0:1, :]]
            sums = [st_in[p, 4 + hm:5 + hm, :] for p in range(3)] + [jnp.sum(l_st[unit], axis=0, keepdims=True)]
            top = functools.reduce(jnp.maximum, peaks)
            powers = [jnp.exp2(v - top) for v in peaks]
            total = sum(v * l for v, l in zip(powers, sums))
            inverse = 1.0 / total
            merged = acc[unit] * (powers[3] * inverse)
            for p in range(3):
                merged += o_in[p, hm * 128:(hm + 1) * 128, :].astype(F32) * (powers[p] * sums[p] * inverse)
            maps.append(merged)
        differ = maps[0] - lam_ref[h] * maps[1]
        mean_square = jnp.mean(differ * differ, axis=0, keepdims=True)
        scaled = jnp.transpose(differ * lax.rsqrt(mean_square + EPSILON))
        att_own[:, h * 128:(h + 1) * 128] = (scaled * hg_ref[...] * 0.8).astype(BF16)
    exchange = [("a", dy, dx) for dy in range(4) for dx in range(4) if dy or dx]
    rows = pl.multiple_of(x * 64, 64)
    keep = pltpu.make_async_copy(att_own.at[pl.ds(rows, 64)], att.at[x, 0:64], local_sems.at[2])
    keep.start()
    start(*exchange)
    w_last(5)()
    w_last(6)()
    w_on(7)()
    keep.wait()
    wo_copy.wait()
    arrive(*exchange)

    def project(n, carry):
        cols = pl.ds(pl.multiple_of(n * 256, 256), 256)
        total = None
        for i in range(4):
            term = jnp.dot(att[i], wo_v[i * 256:(i + 1) * 256, cols], preferred_element_type=F32)
            total = term if total is None else total + term
        branch[:, cols] = total
        return carry

    lax.fori_loop(0, 8, project, 0)
    w_last(7)()
    arrive(("s", 1), ("s", 2), ("s", 3))

    def norm(n, carry):
        r = pl.ds(pl.multiple_of(n * 16, 16), 16)
        j, within = n // 4, pl.ds(pl.multiple_of(lax.rem(n, 4) * 16, 16), 16)
        mixed = ALPHA * s_all[j, within, :].astype(F32) + branch[r, :]
        mean = jnp.mean(mixed, axis=-1, keepdims=True)
        centered = mixed - mean
        var = jnp.mean(centered * centered, axis=-1, keepdims=True)
        normed[r, :] = (centered * lax.rsqrt(var + EPSILON) * ng_ref[...]).astype(BF16)
        return carry

    lax.fori_loop(0, 16, norm, 0)
    for kind in ("wd0", "wd1", "wd2", "wd3"):
        arrive(*[(kind, i) for i in range(8)])
    for lo, hi in ((0, 256), (256, 512), (512, 704)):
        gate = jnp.dot(normed[...], w_all[:, 0:32, lo:hi].reshape(2048, hi - lo), preferred_element_type=F32)
        upward = jnp.dot(normed[...], w_all[:, 32:64, lo:hi].reshape(2048, hi - lo), preferred_element_type=F32)
        hidden[:, lo:hi] = (gate / (1.0 + jnp.exp(-gate)) * upward).astype(BF16)
    for h in range(2):
        def down(n, carry):
            rows_of = pl.ds(pl.multiple_of((h * 4 + n) * 8, 8), 8)
            product = lax.dot_general(
                hidden[...], w_all[rows_of, 64:96, :].reshape(256, 704), (((1,), (1,)), ((), ())),
                preferred_element_type=F32,
            ).astype(BF16)
            cols = pl.ds(pl.multiple_of(n * 256, 256), 256)
            for j in range(4):
                part[h, j, :, cols] = product[j * 64:(j + 1) * 64]
            return carry

        lax.fori_loop(0, 4, down, 0)
        start(("p", h, 2), ("p", h, 1), ("p", h, 3))
    for h in range(2):
        for j in range(1, 4):
            arrive(("p", h, j))
        cols = slice(h * 1024, (h + 1) * 1024)
        mixer = part[h, 0].astype(F32)
        for j in range(1, 4):
            mixer += part_in[h, j].astype(F32)
        out_ref[:, cols] = (ALPHA * normed[0:64, cols].astype(F32) + 0.5 * mixer).astype(BF16)
    for name in NAMES:
        if name != ("t",):
            describe(name).wait_send()

    @pl.when(jnp.logical_not(stays))
    def _():
        describe(("t",)).wait_send()


def on_device(
    stream, query_one, key_one, query_two, key_two, values, lambdas, head_gain, out_weight, norm_gain,
    gate_weight, up_weight, down_weight,
):
    queries = jnp.concatenate([query_one, query_two], axis=1)
    keys = jnp.concatenate([key_one, key_two], axis=1)
    turned = jnp.transpose(values)
    weights = jnp.concatenate([gate_weight, up_weight, jnp.transpose(down_weight)], axis=0)
    vmem = pl.BlockSpec(memory_space=pltpu.VMEM)
    return pl.pallas_call(
        kernel,
        out_shape=jax.ShapeDtypeStruct((64, 2048), BF16),
        in_specs=[vmem] * 5 + [pl.BlockSpec(memory_space=pltpu.SMEM), vmem, vmem, pl.BlockSpec(memory_space=pl.ANY)],
        out_specs=vmem,
        scratch_shapes=[
            pltpu.VMEM((4, 256, 256), BF16),
            pltpu.VMEM((16, 256, 256), BF16),
            pltpu.VMEM((16, 256, 256), BF16),
            pltpu.VMEM((16, 128, 256), F32),
            pltpu.VMEM((16, 8, 256), F32),
            pltpu.VMEM((16, 8, 256), F32),
            pltpu.VMEM((NB * 256, 256), F32),
            pltpu.VMEM((NB * 256, 256), F32),
            pltpu.VMEM((64, 96, 704), BF16),
            pltpu.VMEM((4, 64, 2048), BF16),
            pltpu.VMEM((1024, 2048), BF16),
            pltpu.VMEM((3, 512, 256), BF16),
            pltpu.VMEM((3, 8, 256), F32),
            pltpu.VMEM((3, 512, 256), BF16),
            pltpu.VMEM((3, 8, 256), F32),
            pltpu.VMEM((256, 256), BF16),
            pltpu.VMEM((4, 256, 256), BF16),
            pltpu.VMEM((256, 2048), F32),
            pltpu.VMEM((256, 2048), BF16),
            pltpu.VMEM((256, 704), BF16),
            pltpu.VMEM((2, 4, 64, 1024), BF16),
            pltpu.VMEM((2, 4, 64, 1024), BF16),
            pltpu.SemaphoreType.DMA((len(NAMES),)),
            pltpu.SemaphoreType.DMA((len(NAMES),)),
            pltpu.SemaphoreType.DMA((3,)),
        ],
        compiler_params=pltpu.CompilerParams(
            collective_id=0, has_side_effects=True, vmem_limit_bytes=60 * 2**20
        ),
    )(
        queries, keys, turned, weights, stream, lambdas, head_gain.reshape(1, 128), norm_gain.reshape(1, 2048),
        out_weight,
    )


def solution(mesh):
    return jax.shard_map(
        on_device,
        mesh=mesh,
        in_specs=(
            P(("sp", "tp"), None), P("sp", "tp"), P("sp", "tp"), P("sp", "tp"), P("sp", "tp"), P("sp", "tp"),
            P("tp"), P(), P(), P(), P("sp", "tp"), P("sp", "tp"), P("tp", "sp"),
        ),
        out_specs=P(("sp", "tp"), None),
        check_vma=False,
    )
```

time: 359 us -> 112 us (0.31)
  matrix products: 120 us -> 0 us
  waiting for transfers between devices: 110 us -> 0 us
  Pallas kernels: 0 us -> 105 us
  local copies, waits for them, and re-layouts: 56.2 us -> 3.33 us
  blocking collectives: 23.9 us -> 0 us
  between operations: 13.3 us -> 0.01 us
  other arithmetic: 16.4 us -> 3.18 us
  loops' own time: 11.8 us -> 0 us
  starting transfers between devices: 3.78 us -> 0 us
    dot_general x51 -> x0, matrix products: 120 us -> none  [the longest x16 46.2 us: update(): jnp.einsum('hqk,khe->qhe', weights.astype(jnp.bfloat16), value_rows, pref...]
    pallas_call x0 -> x1, Pallas kernels: none -> 105 us  [on_device(): pl.pallas_call(kernel, out_shape=jax.ShapeDtypeStruct((64, 2048), BF16),...]
    all_gather x3 -> x0, waiting for transfers between devices: 101 us -> none  [the longest x2 101 us: sent_together(): result = lax.all_gather(both, axis, axis=dim, tiled=True)]
    split x5 -> x0, local copies, waits for them, and re-layouts: 37.6 us -> none  [sent_together(): jnp.split(result, [sum(widths[:k]) for k in range(1, len(widths))], axis=...]
    all_to_all x2 -> x0, blocking collectives: 23.9 us -> none  [the longest x1 15.3 us: sum_at_owner(): lax.all_to_all(cut_along(shard, dim, count), axis, 0, 0, tiled=True)]
    another operation x18 -> x0, loops' own time: 11.8 us -> none  [the longest x1 10.7 us: sectioned_absorb(): running = lax.fori_loop(0, filled.shape[0], visit_block, running)]
    reduce_sum x19 -> x0, other arithmetic: 11.7 us -> none  [the longest x16 11.2 us: update(): totals = totals * rescale + jnp.sum(weights, axis=-1)]
    dynamic_slice x16 -> x0, local copies, waits for them, and re-layouts: 9.41 us -> none  [visit_block(): return lax.cond(completed[block_index], compute, unchanged, totals)]
  transfers between devices with their start and end apart: 4 -> 0, of which waited for: 2 -> 0; matrix products, arithmetic and copies ran while one was open for 43% -> 0% of each run, Pallas kernels for 0% -> 0%
where the time goes in v1:
time: 112 us
  Pallas kernels  105 us (94%)
  local copies, waits for them, and re-layouts  3.33 us (3%)
  other arithmetic  3.18 us (3%)
    pallas_call x1, Pallas kernels, on_device(): pl.pallas_call(kernel, out_shape=jax.ShapeDtypeStruct((64, 2048), BF16),...  105 us
    unnamed x2, local copies, waits for them, and re-layouts  3.33 us

profile of v1, /device:TPU:1, one launch (start us, length us, event | category | flops | bytes accessed | tf_op | source)
XLA Modules:
  0.0 112.0 jit_solution(6000241587257912061)
XLA Ops:
  0.0 1.7 %copy.14 = bf16[256,256]{0,1:T(8,128)(2,1)} copy(bf16[256,256]{1,0:T(8,128)(2,1)} %param.18) | data formatting | bytes 262144 | tf_op args[5]
  1.7 1.5 %pad_maximum_fusion.w_ref = bf16[96,704]{1,0:T(8,128)(2,1)} fusion(bf16[32,704]{1,0:T(8,128)(2,1)} %bitcast.5, bf16[32,704]{1,0:T(8,128)(2,1)} %param.24, bf16[32,704]{1,0:T(8,128)(2,1)} %param.23), kind=kLoop, calls=%fused_computation | loop fusion | flops 405504 | bytes 270336 | tf_op jit(solution)/shard_map/concatenate | solution.py:436
  3.2 1.7 %pad_maximum_fusion.1 = (bf16[256,256]{1,0:T(8,128)(2,1)}, bf16[256,256]{1,0:T(8,128)(2,1)}) fusion(bf16[256,128]{1,0:T(8,128)(2,1)} %param.16, bf16[256,128]{1,0:T(8,128)(2,1)} %param.14, bf16[256,128]{1,0:T(8,128)(2,1)} %param.17, bf16[256,128]{1,0:T(8,128)(2,1)} %param.15), kind=kLoop, calls=%fused_computation.1 | loop fusion | flops 524288 | bytes 524288 | tf_op jit(solution)/shard_map/concatenate | solution.py:433
  4.8 105.5 %shard_map.127 = bf16[64,2048]{1,0:T(8,128)(2,1)} custom-call(bf16[256,256]{1,0:T(8,128)(2,1)} %get-tuple-element.5.q_ref, bf16[256,256]{1,0:T(8,128)(2,1)} %get-tuple-element.6.k_ref, bf16[256,256]{1,0:T(8,128)(2,1)} %bitcast.4, bf16[96,704]{1,0:T(8,128)(2,1)} %pad_maximum_fusion.w_ref, bf16[64,2048]{1,0:T(8,128)(2,1)} %s_ref.1, f32[2]{0:T(128)} %lam_ref.1, ...), custom_call_target="tpu_custom_call" | custom-call | tf_op jit(solution)/shard_map/pallas_call | solution.py:438
  110.3 1.7 %copy.16 = bf16[64,2048]{1,0:T(8,128)(2,1)} copy(bf16[64,2048]{1,0:T(8,128)(2,1)} %shard_map.127) | data formatting | bytes 524288

commit v2 on v1

--- a/solution.py
+++ b/solution.py
@@ -14,17 +14,9 @@
 ALPHA = 1.4142135623730951
 EPSILON = 1e-05
 SCALE = math.log2(math.e) / 8.0
-NB = 4
+NB = 2
 REL = (2, 1, 3, 0)
 Z_OF_SLOT = (0, -1, 1, -2, 2, -3, 3, 4)
-
-
-class Messages:
-    def __init__(self):
-        self.index = {}
-
-    def of(self, name):
-        return self.index.setdefault(name, len(self.index))
 
 
 def message_names():
@@ -46,10 +38,10 @@
 
 
 def kernel(
-    q_ref, k_ref, v_ref, w_ref, s_ref, lam_ref, hg_ref, ng_ref, wo_ref,
+    q1_ref, q2_ref, k1_ref, k2_ref, v_ref, g_ref, u_ref, d_ref, s_ref, lam_ref, hg_ref, ng_ref, wo_ref,
     out_ref,
-    q_all, k_all, v_all, acc, m_st, l_st, sb0, sb1, w_all, s_all, wo_v,
-    o_out, st_out, o_in, st_in, att_own, att, branch, normed, hidden, part, part_in,
+    q_all, k_all, v_all, acc, m_st, l_st, sb0, sb1, w_own, w_all, s_all, wo_v,
+    o_out, st_out, o_in, st_in, att_own, att, branch, row_sums, normed, hidden, part, part_in,
     send_sems, recv_sems, local_sems,
 ):
     sp = lax.axis_index("sp")
@@ -81,22 +73,21 @@
         kind = name[0]
         if kind == "q":
             p = name[1]
-            return remote(name, q_ref, q_all.at[p], at(dy=REL[p]))
+            return remote(name, q_all.at[3], q_all.at[p], at(dy=REL[p]))
         if kind in ("k", "v"):
             s = name[1]
-            buf, own = (k_all, k_ref) if kind == "k" else (v_all, v_ref)
+            buf = k_all if kind == "k" else v_all
             step = 1 if s in (1, 3, 5) else -1
             before = s - 2
             if s == 7:
                 step, before = (1, 5) if kind == "k" else (-1, 6)
-            src = own if s <= 2 else buf.at[2 * before]
-            return remote(name, src, buf.at[2 * s], at(dz=step))
+            return remote(name, buf.at[2 * max(before, 0)], buf.at[2 * s], at(dz=step))
         if kind in ("kd", "vd"):
             s = name[1]
-            buf, own = (k_all, k_ref) if kind == "kd" else (v_all, v_ref)
-            return remote(name, own if s == 0 else buf.at[2 * s], buf.at[2 * s + 1], at(dc=1))
+            buf = k_all if kind == "kd" else v_all
+            return remote(name, buf.at[2 * s], buf.at[2 * s + 1], at(dc=1))
         if kind == "t":
-            return remote(name, w_ref, w_all.at[z * 8 + y * 2 + c], {"sp": z * 8 + x * 2 + c, "tp": y})
+            return remote(name, w_own, w_all.at[z * 8 + y * 2 + c], {"sp": z * 8 + x * 2 + c, "tp": y})
         if kind == "wz":
             s = name[1]
             step = 1 if s in (1, 3, 5) else -1
@@ -154,16 +145,21 @@
         pl.semaphore_signal(barrier, inc=1, device_id=partner, device_id_type=MESH)
     wo_copy = pltpu.make_async_copy(wo_ref, wo_v, local_sems.at[0])
     wo_copy.start()
-    q_all[3] = q_ref[...]
-    k_all[0] = k_ref[...]
-    v_all[0] = v_ref[...]
+    q_all[3, :, 0:128] = q1_ref[...]
+    q_all[3, :, 128:256] = q2_ref[...]
+    k_all[0, :, 0:128] = k1_ref[...]
+    k_all[0, :, 128:256] = k2_ref[...]
+    v_all[0] = jnp.transpose(v_ref[...])
+    w_own[0:32] = g_ref[...]
+    w_own[32:64] = u_ref[...]
+    w_own[64:96] = d_ref[...]
     s_all[0] = s_ref[...]
     m_st[...] = jnp.full_like(m_st, -1e30)
     l_st[...] = jnp.zeros_like(l_st)
     acc[...] = jnp.zeros_like(acc)
     pl.semaphore_wait(barrier, len(partners))
 
-    own_w = pltpu.make_async_copy(w_ref, w_all.at[z * 8 + y * 2 + c], local_sems.at[1])
+    own_w = pltpu.make_async_copy(w_own, w_all.at[z * 8 + y * 2 + c], local_sems.at[1])
     stays = x == y
     start(("q", 0), ("k", 1), ("k", 2), ("kd", 0), ("v", 1), ("v", 2), ("vd", 0), ("q", 1), ("q", 2))
 
@@ -175,25 +171,18 @@
     def _():
         start(("t",))
 
-    @pl.when(stays)
-    def _():
-        own_w.wait()
-
-    @pl.when(jnp.logical_not(stays))
-    def _():
-        arrive(("t",))
-
-    start(("wxl", 0), ("wxr", 0), ("wd0", 0))
-    arrive(("q", 0), ("kd", 0), ("vd", 0), ("k", 1))
-    start(("k", 3), ("kd", 1))
-    arrive(("k", 2))
-    start(("k", 4), ("kd", 2))
-    arrive(("v", 1))
-    start(("v", 3), ("vd", 1))
-    arrive(("v", 2))
-    start(("v", 4), ("vd", 2))
-    start(("wz", 1), ("wz", 2))
-    arrive(("kd", 1), ("vd", 1))
+    arrive(("q", 0), ("kd", 0), ("vd", 0))
+
+    def w_in():
+        @pl.when(stays)
+        def _():
+            own_w.wait()
+
+        @pl.when(jnp.logical_not(stays))
+        def _():
+            arrive(("t",))
+
+        start(("wz", 1), ("wz", 2))
 
     def w_across(i):
         def act():
@@ -212,26 +201,22 @@
             start(("wd3", i))
         return act
 
-    def ring_on(s):
-        def act():
-            for a in "kv":
-                arrive((a, s), (a, s + 1))
-                if s < 5:
-                    start((a, s + 2), (a, s + 3))
-                else:
-                    start((a, 7))
-                start((a + "d", s), (a + "d", s + 1))
+    def on(a, s):
+        def act():
+            arrive((a, s), (a, s + 1))
+            if s < 5:
+                start((a, s + 2), (a, s + 3))
+            else:
+                start((a, 7))
+            start((a + "d", s), (a + "d", s + 1))
         return act
 
     def ring_end():
         arrive(("k", 7), ("v", 7))
         start(("kd", 7), ("vd", 7))
 
-    def copies(*slots):
-        def act():
-            for s in slots:
-                arrive(("kd", s), ("vd", s))
-        return act
+    def got(*names):
+        return lambda: arrive(*names)
 
     def w_ring(s):
         def act():
@@ -240,6 +225,8 @@
                 start(("wz", s + 2), ("wz", s + 3))
             else:
                 start(("wz7a",), ("wz7b",))
+            w_across(s)()
+            w_across(s + 1)()
         return act
 
     def w_ring_end():
@@ -257,19 +244,26 @@
         return act
 
     events = {
-        0: [lambda: arrive(("q", 1))],
-        1: [lambda: arrive(("q", 2)), lambda: start(("s", 1), ("s", 3), ("s", 2))],
-        2: [w_on(0)],
-        3: [ring_on(3), copies(2, 3)],
-        4: [w_ring(1), w_across(1), w_across(2), w_last(0)],
-        7: [ring_on(5), copies(4, 5), w_on(1), w_on(2)],
-        8: [w_ring(3), w_across(3), w_across(4)],
-        10: [w_last(1), w_last(2)],
-        11: [ring_end, copies(6, 7), w_on(3), w_on(4)],
-        12: [w_ring(5), w_across(5), w_across(6)],
-        13: [finalize(0), w_last(3), w_last(4)],
-        14: [finalize(1)],
-        15: [finalize(2), w_on(5), w_on(6)],
+        0: [got(("q", 1))],
+        1: [got(("q", 2)), on("k", 1)],
+        2: [lambda: start(("s", 1), ("s", 3), ("s", 2))],
+        3: [on("v", 1), got(("kd", 1))],
+        4: [got(("vd", 1)), w_in, w_across(0)],
+        7: [got(("kd", 2), ("vd", 2)), on("k", 3)],
+        10: [on("v", 3)],
+        11: [got(("kd", 3), ("vd", 3))],
+        12: [w_on(0)],
+        15: [w_ring(1), got(("kd", 4), ("vd", 4))],
+        18: [on("k", 5)],
+        19: [on("v", 5), got(("kd", 5), ("vd", 5))],
+        20: [w_last(0)],
+        22: [w_on(1)],
+        23: [got(("kd", 6), ("vd", 6)), ring_end],
+        24: [got(("kd", 7), ("vd", 7)), w_on(2)],
+        26: [finalize(0)],
+        27: [w_ring(3), w_last(1)],
+        28: [finalize(1)],
+        30: [finalize(2), w_last(2)],
     }
 
     def scores(s_buf, qi, hm, first):
@@ -309,6 +303,11 @@
         acc[unit] = (acc[unit].reshape(16, 8, 256) * rescale[None] + out.reshape(16, 8, 256)).reshape(128, 256)
 
     bufs = (sb0, sb1)
+
+    def place(t):
+        late = t >= 24
+        return jnp.where(late, 6 + lax.rem(t, 2), t // 4), jnp.where(late, (t - 24) // 2, lax.rem(t, 4))
+
     first_peak = scores(bufs[0], 0, 0, 0)
 
     def body(t, peak):
@@ -317,23 +316,25 @@
             def _(actions=actions):
                 for action in actions:
                     action()
-        step, qi = t // 4, lax.rem(t, 4)
-        later = jnp.minimum(t + 1, 15)
+        slot, qi = place(t)
+        slot_ahead, qi_ahead = place(jnp.minimum(t + 1, 31))
         for hm in range(4):
             if hm < 3:
-                ahead = scores(bufs[(hm + 1) % 2], qi, hm + 1, step * NB)
+                ahead = scores(bufs[(hm + 1) % 2], qi, hm + 1, slot * NB)
             else:
-                ahead = scores(bufs[0], lax.rem(later, 4), 0, (later // 4) * NB)
-            absorb(bufs[hm % 2], qi * 4 + hm, hm, step * NB, peak)
+                ahead = scores(bufs[0], qi_ahead, 0, slot_ahead * NB)
+            absorb(bufs[hm % 2], qi * 4 + hm, hm, slot * NB, peak)
             peak = ahead
         return peak
 
-    lax.fori_loop(0, 16, body, first_peak)
-
-    w_ring_end()
-    w_across(7)()
-    for p in range(3):
-        arrive(("o", p), ("st", p))
+    lax.fori_loop(0, 32, body, first_peak)
+
+    arrive(("o", 0), ("st", 0))
+    w_ring(5)()
+    arrive(("o", 1), ("st", 1))
+    w_on(3)()
+    w_on(4)()
+    arrive(("o", 2), ("st", 2))
     for h in range(2):
         maps = []
         for m in range(2):
@@ -358,37 +359,46 @@
     keep = pltpu.make_async_copy(att_own.at[pl.ds(rows, 64)], att.at[x, 0:64], local_sems.at[2])
     keep.start()
     start(*exchange)
-    w_last(5)()
-    w_last(6)()
-    w_on(7)()
+    w_ring_end()
+    w_across(7)()
+    w_last(3)()
+    w_last(4)()
+    w_on(5)()
+    w_on(6)()
     keep.wait()
     wo_copy.wait()
     arrive(*exchange)
 
+    arrive(("s", 1), ("s", 2), ("s", 3))
+    row_sums[...] = jnp.zeros_like(row_sums)
+
     def project(n, carry):
-        cols = pl.ds(pl.multiple_of(n * 256, 256), 256)
+        cols = pl.ds(pl.multiple_of(n * 512, 512), 512)
         total = None
         for i in range(4):
             term = jnp.dot(att[i], wo_v[i * 256:(i + 1) * 256, cols], preferred_element_type=F32)
             total = term if total is None else total + term
-        branch[:, cols] = total
+        mixed = ALPHA * s_all[:, :, cols].reshape(256, 512).astype(F32) + total
+        branch[:, cols] = mixed
+        row_sums[...] += sum(mixed[:, i * 128:(i + 1) * 128] for i in range(4))
         return carry
 
-    lax.fori_loop(0, 8, project, 0)
+    lax.fori_loop(0, 4, project, 0)
+    w_last(5)()
+    w_last(6)()
+    w_on(7)()
+    mean = jnp.sum(row_sums[...], axis=-1, keepdims=True) * (1.0 / 2048)
+    row_sums[...] = jnp.broadcast_to(mean, (256, 128))
+    spread = None
+    for n in range(16):
+        centered = branch[:, n * 128:(n + 1) * 128] - row_sums[...]
+        spread = centered * centered if spread is None else spread + centered * centered
+    var = jnp.sum(spread, axis=-1, keepdims=True) * (1.0 / 2048)
+    inverse = jnp.broadcast_to(lax.rsqrt(var + EPSILON), (256, 128))
+    for n in range(16):
+        cols = slice(n * 128, (n + 1) * 128)
+        normed[:, cols] = ((branch[:, cols] - row_sums[...]) * inverse * ng_ref[:, cols]).astype(BF16)
     w_last(7)()
-    arrive(("s", 1), ("s", 2), ("s", 3))
-
-    def norm(n, carry):
-        r = pl.ds(pl.multiple_of(n * 16, 16), 16)
-        j, within = n // 4, pl.ds(pl.multiple_of(lax.rem(n, 4) * 16, 16), 16)
-        mixed = ALPHA * s_all[j, within, :].astype(F32) + branch[r, :]
-        mean = jnp.mean(mixed, axis=-1, keepdims=True)
-        centered = mixed - mean
-        var = jnp.mean(centered * centered, axis=-1, keepdims=True)
-        normed[r, :] = (centered * lax.rsqrt(var + EPSILON) * ng_ref[...]).astype(BF16)
-        return carry
-
-    lax.fori_loop(0, 16, norm, 0)
     for kind in ("wd0", "wd1", "wd2", "wd3"):
         arrive(*[(kind, i) for i in range(8)])
     for lo, hi in ((0, 256), (256, 512), (512, 704)):
@@ -430,15 +440,11 @@
     stream, query_one, key_one, query_two, key_two, values, lambdas, head_gain, out_weight, norm_gain,
     gate_weight, up_weight, down_weight,
 ):
-    queries = jnp.concatenate([query_one, query_two], axis=1)
-    keys = jnp.concatenate([key_one, key_two], axis=1)
-    turned = jnp.transpose(values)
-    weights = jnp.concatenate([gate_weight, up_weight, jnp.transpose(down_weight)], axis=0)
     vmem = pl.BlockSpec(memory_space=pltpu.VMEM)
     return pl.pallas_call(
         kernel,
         out_shape=jax.ShapeDtypeStruct((64, 2048), BF16),
-        in_specs=[vmem] * 5 + [pl.BlockSpec(memory_space=pltpu.SMEM), vmem, vmem, pl.BlockSpec(memory_space=pl.ANY)],
+        in_specs=[vmem] * 9 + [pl.BlockSpec(memory_space=pltpu.SMEM), vmem, vmem, pl.BlockSpec(memory_space=pl.ANY)],
         out_specs=vmem,
         scratch_shapes=[
             pltpu.VMEM((4, 256, 256), BF16),
@@ -449,6 +455,7 @@
             pltpu.VMEM((16, 8, 256), F32),
             pltpu.VMEM((NB * 256, 256), F32),
             pltpu.VMEM((NB * 256, 256), F32),
+            pltpu.VMEM((96, 704), BF16),
             pltpu.VMEM((64, 96, 704), BF16),
             pltpu.VMEM((4, 64, 2048), BF16),
             pltpu.VMEM((1024, 2048), BF16),
@@ -459,6 +466,7 @@
             pltpu.VMEM((256, 256), BF16),
             pltpu.VMEM((4, 256, 256), BF16),
             pltpu.VMEM((256, 2048), F32),
+            pltpu.VMEM((256, 128), F32),
             pltpu.VMEM((256, 2048), BF16),
             pltpu.VMEM((256, 704), BF16),
             pltpu.VMEM((2, 4, 64, 1024), BF16),
@@ -471,7 +479,7 @@
             collective_id=0, has_side_effects=True, vmem_limit_bytes=60 * 2**20
         ),
     )(
-        queries, keys, turned, weights, stream, lambdas, head_gain.reshape(1, 128), norm_gain.reshape(1, 2048),
+        query_one, query_two, key_one, key_two, values, gate_weight, up_weight, jnp.transpose(down_weight), stream, lambdas, head_gain.reshape(1, 128), norm_gain.reshape(1, 2048),
         out_weight,
     )
 

time: 112 us -> 121 us (1.080)
  Pallas kernels: 105 us -> 119 us
  other arithmetic: 3.18 us -> 0 us
  local copies, waits for them, and re-layouts: 3.33 us -> 1.67 us
    pallas_call x1, Pallas kernels: 105 us -> 119 us  [on_device(): pl.pallas_call(kernel, out_shape=jax.ShapeDtypeStruct((64, 2048), BF16),...]
    concatenate x2 -> x0, other arithmetic: 3.18 us -> none  [the longest x1 1.66 us: on_device(): queries = jnp.concatenate([query_one, query_two], axis=1)]
    unnamed x2 -> x1, local copies, waits for them, and re-layouts: 3.33 us -> 1.67 us
where the time goes in v2:
time: 121 us
  Pallas kernels  119 us (98%)
  local copies, waits for them, and re-layouts  1.67 us (1%)
    pallas_call x1, Pallas kernels, on_device(): pl.pallas_call(kernel, out_shape=jax.ShapeDtypeStruct((64, 2048), BF16),...  119 us

profile of v2, /device:TPU:1, one launch (start us, length us, event | category | flops | bytes accessed | tf_op | source)
XLA Modules:
  0.0 120.8 jit_solution(14639392634759711844)
XLA Ops:
  0.0 119.1 %shard_map.127 = bf16[64,2048]{1,0:T(8,128)(2,1)} custom-call(bf16[256,128]{1,0:T(8,128)(2,1)} %q1_ref.1, bf16[256,128]{1,0:T(8,128)(2,1)} %q2_ref.1, bf16[256,128]{1,0:T(8,128)(2,1)} %k1_ref.1, bf16[256,128]{1,0:T(8,128)(2,1)} %k2_ref.1, bf16[256,256]{1,0:T(8,128)(2,1)} %v_ref.1, bf16[32,704]{1,0:T(8,128)(2,1)} %g_ref.1, bf16[32,704]{1,0:T(8,128)(2,1)} %u_ref.1, ...), custom_call_target="tpu_custom_call" | custom-call | tf_op jit(solution)/shard_map/pallas_call | solution.py:444
  119.1 1.7 %copy.15 = bf16[64,2048]{1,0:T(8,128)(2,1)} copy(bf16[64,2048]{1,0:T(8,128)(2,1)} %shard_map.127) | data formatting | bytes 524288

commit v3 on v2

v3 whole, which is shorter than its diff:
```python
import functools
import math

import jax
import jax.numpy as jnp
from jax import lax
from jax.experimental import pallas as pl
from jax.experimental.pallas import tpu as pltpu
from jax.sharding import PartitionSpec as P

MESH = pl.DeviceIdType.MESH
F32 = jnp.float32
BF16 = jnp.bfloat16
ALPHA = 1.4142135623730951
EPSILON = 1e-05
SCALE = math.log2(math.e) / 8.0
REL = (0, 1, 3, 2)
Z_OF_SLOT = (0, -1, 1, -2, 2, -3, 3, 4)


def message_names():
    names = [("q", p) for p in range(1, 4)]
    for a in "kv":
        names += [(a, s) for s in range(1, 8)] + [(a + "d", s) for s in range(8)]
    names += [("wz", s) for s in range(1, 7)] + [("wz7a",), ("wz7b",)]
    for kind in ("wxl", "wxr", "wxa", "wxb", "wd0", "wd1", "wd2", "wd3"):
        names += [(kind, i) for i in range(8)]
    names += [("s", j) for j in range(1, 4)]
    names += [("o", p) for p in range(1, 4)] + [("st", p) for p in range(1, 4)]
    names += [("a", j) for j in range(1, 4)]
    names += [("p", h, j) for h in range(2) for j in range(1, 4)]
    return names


NAMES = message_names()
INDEX = {name: i for i, name in enumerate(NAMES)}


def kernel(
    q1_ref, q2_ref, k1_ref, k2_ref, v_ref, g_ref, u_ref, d_ref, s_ref, lam_ref, hg_ref, ng_ref, wo_ref,
    out_ref,
    q_all, k_all, v_all, v_own, acc, m_st, l_st, sb0, sb1, w_all, s_all, wo_v,
    o_out, st_out, o_in, st_in, att, branch, row_sums, normed, hidden, part, part_in,
    send_sems, recv_sems, local_sems,
):
    sp = lax.axis_index("sp")
    x = lax.axis_index("tp")
    z = sp // 8
    y = lax.rem(sp, 8) // 2
    c = lax.rem(sp, 2)

    def mod(a, n):
        return lax.rem(a + 2 * n, n)

    def at(dz=0, dy=0, dc=0, dx=0):
        return {
            "sp": mod(z + dz, 8) * 8 + mod(y + dy, 4) * 2 + mod(c + dc, 2),
            "tp": mod(x + dx, 4),
        }

    def block(dz=0, dy=0):
        return mod(z + dz, 8) * 8 + mod(y + dy, 4) * 2 + c

    def remote(name, src, dst, target):
        i = INDEX[name]
        return pltpu.make_async_remote_copy(
            src_ref=src, dst_ref=dst, send_sem=send_sems.at[i], recv_sem=recv_sems.at[i],
            device_id=target, device_id_type=MESH,
        )

    def describe(name):
        kind = name[0]
        if kind == "q":
            p = name[1]
            return remote(name, q_all.at[0], q_all.at[p], at(dy=REL[p]))
        if kind in ("k", "v"):
            s = name[1]
            buf = k_all if kind == "k" else v_all
            step = 1 if s in (1, 3, 5) else -1
            before = s - 2
            if s == 7:
                step, before = (1, 5) if kind == "k" else (-1, 6)
            return remote(name, buf.at[2 * max(before, 0)], buf.at[2 * s], at(dz=step))
        if kind in ("kd", "vd"):
            s = name[1]
            buf = k_all if kind == "kd" else v_all
            return remote(name, buf.at[2 * s], buf.at[2 * s + 1], at(dc=1))
        if kind == "wz":
            s = name[1]
            step = 1 if s in (1, 3, 5) else -1
            ref = w_all.at[block(dz=Z_OF_SLOT[s - 2] if s > 2 else 0)]
            return remote(name, ref, ref, at(dz=step))
        if kind == "wz7a":
            ref = w_all.at[block(dz=-3), 0:48]
            return remote(name, ref, ref, at(dz=1))
        if kind == "wz7b":
            ref = w_all.at[block(dz=3), 48:96]
            return remote(name, ref, ref, at(dz=-1))
        if kind in ("wxl", "wxr"):
            ref = w_all.at[block(dz=Z_OF_SLOT[name[1]])]
            return remote(name, ref, ref, at(dy=1 if kind == "wxl" else -1))
        if kind == "wxa":
            ref = w_all.at[block(dz=Z_OF_SLOT[name[1]], dy=-1), 0:48]
            return remote(name, ref, ref, at(dy=1))
        if kind == "wxb":
            ref = w_all.at[block(dz=Z_OF_SLOT[name[1]], dy=1), 48:96]
            return remote(name, ref, ref, at(dy=-1))
        if kind[:2] == "wd":
            ref = w_all.at[block(dz=Z_OF_SLOT[name[1]], dy=(0, -1, 1, 2)[int(kind[2])])]
            return remote(name, ref, ref, at(dc=1))
        if kind == "s":
            return remote(name, s_all.at[x], s_all.at[x], at(dx=name[1]))
        if kind == "o":
            p = name[1]
            return remote(name, o_out.at[p - 1], o_in.at[p - 1], at(dy=-REL[p]))
        if kind == "st":
            p = name[1]
            return remote(name, st_out.at[p - 1], st_in.at[p - 1], at(dy=-REL[p]))
        if kind == "a":
            return remote(name, att.at[x], att.at[x], at(dx=name[1]))
        if kind == "p":
            h, j = name[1:]
            rows = pl.multiple_of(mod(x - j, 4) * 64, 64)
            return remote(name, part.at[h, pl.ds(rows, 64)], part_in.at[h, j], at(dx=-j))
        raise KeyError(kind)

    def start(*names):
        for name in names:
            describe(name).start()

    def arrive(*names):
        for name in names:
            describe(name).wait_recv()

    barrier = pltpu.get_barrier_semaphore()
    partners = [at(dz=1), at(dz=-1), at(dc=1)]
    partners += [at(dy=j) for j in range(1, 4)] + [at(dx=j) for j in range(1, 4)]
    for partner in partners:
        pl.semaphore_signal(barrier, inc=1, device_id=partner, device_id_type=MESH)
    takes = [
        pltpu.make_async_copy(src, dst, local_sems.at[3 + i])
        for i, (src, dst) in enumerate((
            (v_ref, v_own), (q1_ref, q_all.at[0, :, 0:128]), (q2_ref, q_all.at[0, :, 128:256]),
            (k1_ref, k_all.at[0, :, 0:128]), (k2_ref, k_all.at[0, :, 128:256]),
            (g_ref, w_all.at[sp, 0:32]), (u_ref, w_all.at[sp, 32:64]), (d_ref, w_all.at[sp, 64:96]), (s_ref, s_all.at[x]),
        ))
    ]
    for take in takes:
        take.start()
    wo_copy = pltpu.make_async_copy(wo_ref, wo_v, local_sems.at[0])
    wo_copy.start()
    m_st[...] = jnp.full_like(m_st, -1e30)
    l_st[...] = jnp.zeros_like(l_st)
    acc[...] = jnp.zeros_like(acc)
    takes[0].wait()
    v_all[0] = jnp.transpose(v_own[...])
    for take in takes[1:]:
        take.wait()
    pl.semaphore_wait(barrier, len(partners))

    start(("q", 1), ("q", 2), ("kd", 0), ("k", 1), ("k", 2), ("vd", 0), ("v", 1), ("v", 2), ("q", 3))

    def w_across(i):
        def act():
            start(("wxl", i), ("wxr", i), ("wd0", i))
        return act

    def w_on(i):
        def act():
            arrive(("wxl", i), ("wxr", i))
            start(("wxa", i), ("wxb", i), ("wd1", i), ("wd2", i))
        return act

    def w_last(i):
        def act():
            arrive(("wxa", i), ("wxb", i))
            start(("wd3", i))
        return act

    def on(a, s):
        def act():
            arrive((a, s), (a, s + 1))
            if s < 5:
                start((a, s + 2), (a, s + 3))
            else:
                start((a, 7))
            start((a + "d", s), (a + "d", s + 1))
        return act

    def ring_end():
        arrive(("k", 7), ("v", 7))
        start(("kd", 7), ("vd", 7))

    def got(*names):
        return lambda: arrive(*names)

    def w_ring(s):
        def act():
            arrive(("wz", s), ("wz", s + 1))
            w_across(s)()
            w_across(s + 1)()
        return act

    def w_next(s):
        def act():
            if s < 5:
                start(("wz", s + 2), ("wz", s + 3))
            else:
                start(("wz7a",), ("wz7b",))
        return act

    def w_ring_end():
        arrive(("wz7a",), ("wz7b",))

    def finalize(p):
        def act():
            for hm in range(4):
                unit = p * 4 + hm
                total = jnp.sum(l_st[unit], axis=0, keepdims=True)
                o_out[p - 1, hm * 128:(hm + 1) * 128, :] = (acc[unit] * (1.0 / total)).astype(BF16)
                st_out[p - 1, hm:hm + 1, :] = m_st[unit, 0:1, :]
                st_out[p - 1, 4 + hm:5 + hm, :] = total
            start(("o", p), ("st", p))
        return act

    phases = (
        (0, 2, (
            (got(("kd", 0), ("vd", 0)),),
            (got(("q", 2)), on("k", 1), lambda: start(("wz", 1), ("wz", 2)), w_across(0)),
            (got(("q", 3)), on("v", 1)),
            (got(("kd", 1), ("kd", 2)),),
        )),
        (2, 4, (
            (got(("vd", 1), ("vd", 2)), lambda: start(("s", 1), ("s", 3), ("s", 2))),
            (on("k", 3), w_on(0)),
            (w_ring(1), w_next(1)),
            (on("v", 3), got(("kd", 3), ("kd", 4))),
        )),
        (6, 4, (
            (got(("vd", 3), ("vd", 4)),),
            (w_last(0),),
            (on("k", 5),),
            (got(("kd", 5), ("kd", 6)), w_on(1)),
        )),
        (10, 4, (
            (on("v", 5), w_ring(3), got(("vd", 5), ("vd", 6))),
            (w_on(2),),
            (w_last(1), w_next(3)),
            (ring_end, got(("kd", 7))),
        )),
        (14, 2, (
            (got(("vd", 7)), w_on(3)),
            (finalize(3), w_last(2)),
            (finalize(2),),
            (finalize(1), w_on(4)),
        )),
    )

    def scores(s_buf, qi, hm, first, count):
        m, h = hm // 2, hm % 2
        q = q_all[qi, :, m * 128:(m + 1) * 128]
        lane = lax.broadcasted_iota(jnp.int32, q.shape, 1)
        q = jnp.where((lane >= 64) if h else (lane < 64), q, jnp.zeros_like(q))
        peak = None
        for b in range(count):
            s = lax.dot_general(
                k_all[first + b, :, m * 128:(m + 1) * 128], q, (((1,), (1,)), ((), ())),
                preferred_element_type=F32,
            )
            s_buf[b * 256:(b + 1) * 256, :] = s
            r = jnp.max(s.reshape(32, 8, 256), axis=0)
            peak = r if peak is None else jnp.maximum(peak, r)
        return peak

    def absorb(s_buf, unit, hm, first, count, peak):
        h = hm % 2
        m_old = m_st[unit]
        m_new = jnp.maximum(m_old, jnp.max(peak, axis=0, keepdims=True) * SCALE)
        rescale = jnp.exp2(m_old - m_new)
        m_st[unit] = m_new
        total, out = None, None
        for b in range(count):
            s = s_buf[b * 256:(b + 1) * 256, :].reshape(32, 8, 256)
            weights = jnp.exp2(s * SCALE - m_new[None])
            t = jnp.sum(weights, axis=0)
            total = t if total is None else total + t
            o = jnp.dot(
                v_all[first + b, h * 128:(h + 1) * 128, :], weights.reshape(256, 256).astype(BF16),
                preferred_element_type=F32,
            )
            out = o if out is None else out + o
        l_st[unit] = l_st[unit] * rescale + total
        acc[unit] = (acc[unit].reshape(16, 8, 256) * rescale[None] + out.reshape(16, 8, 256)).reshape(128, 256)

    bufs = (sb0, sb1)

    def visit(qi, first, count, peak, qi_ahead, first_ahead, count_ahead):
        for hm in range(4):
            if hm < 3:
                ahead = scores(bufs[(hm + 1) % 2], qi, hm + 1, first, count)
            else:
                ahead = scores(bufs[0], qi_ahead, 0, first_ahead, count_ahead)
            absorb(bufs[hm % 2], qi * 4 + hm, hm, first, count, peak)
            peak = ahead
        return peak

    peak = None
    for n, (first, count, actions) in enumerate(phases):
        closing = n == len(phases) - 1
        for action in actions[0]:
            action()
        if peak is None:
            peak = scores(bufs[0], 0, 0, first, count)
            visit(0, first, count, peak, 0, first, count)
            arrive(("q", 1))
            peak = scores(bufs[0], 1, 0, first, count)

        def body(i, peak):
            for at_step in (1, 2):
                if actions[at_step]:
                    @pl.when(i == at_step)
                    def _():
                        for action in actions[at_step]:
                            action()
            qi = 3 - i if closing else i
            return visit(qi, first, count, peak, qi - 1 if closing else qi + 1, first, count)

        peak = lax.fori_loop(0 if n else 1, 3, body, peak)
        for action in actions[3]:
            action()
        if closing:
            visit(0, first, count, peak, 0, first, count)
        else:
            ahead = phases[n + 1]
            opening = 3 if n + 2 == len(phases) else 0
            peak = visit(3, first, count, peak, opening, ahead[0], ahead[1])

    w_last(3)()
    w_ring(5)()
    w_next(5)()
    arrive(("o", 3), ("st", 3))
    arrive(("o", 2), ("st", 2))
    arrive(("o", 1), ("st", 1))
    for h in range(2):
        maps = []
        for m in range(2):
            hm = m * 2 + h
            unit = hm
            peaks = [st_in[p, hm:hm + 1, :] for p in range(3)] + [m_st[unit, 0:1, :]]
            sums = [st_in[p, 4 + hm:5 + hm, :] for p in range(3)] + [jnp.sum(l_st[unit], axis=0, keepdims=True)]
            top = functools.reduce(jnp.maximum, peaks)
            powers = [jnp.exp2(v - top) for v in peaks]
            total = sum(v * l for v, l in zip(powers, sums))
            inverse = 1.0 / total
            merged = acc[unit] * (powers[3] * inverse)
            for p in range(3):
                merged += o_in[p, hm * 128:(hm + 1) * 128, :].astype(F32) * (powers[p] * sums[p] * inverse)
            maps.append(merged)
        differ = maps[0] - lam_ref[h] * maps[1]
        mean_square = jnp.mean(differ * differ, axis=0, keepdims=True)
        scaled = jnp.transpose(differ * lax.rsqrt(mean_square + EPSILON))
        att[x, :, h * 128:(h + 1) * 128] = (scaled * hg_ref[...] * 0.8).astype(BF16)
    exchange = [("a", 2), ("a", 1), ("a", 3)]
    start(*exchange)
    w_ring_end()
    w_across(7)()
    w_last(4)()
    w_on(5)()
    w_on(6)()
    wo_copy.wait()
    arrive(*exchange)

    arrive(("s", 1), ("s", 2), ("s", 3))
    row_sums[...] = jnp.zeros_like(row_sums)

    def project(n, carry):
        cols = pl.ds(pl.multiple_of(n * 512, 512), 512)
        total = None
        for i in range(4):
            term = jnp.dot(att[i], wo_v[i * 256:(i + 1) * 256, cols], preferred_element_type=F32)
            total = term if total is None else total + term
        mixed = ALPHA * s_all[:, :, cols].reshape(256, 512).astype(F32) + total
        branch[:, cols] = mixed
        row_sums[...] += sum(mixed[:, i * 128:(i + 1) * 128] for i in range(4))
        return carry

    lax.fori_loop(0, 4, project, 0)
    w_last(5)()
    w_last(6)()
    w_on(7)()
    mean = jnp.sum(row_sums[...], axis=-1, keepdims=True) * (1.0 / 2048)
    row_sums[...] = jnp.broadcast_to(mean, (256, 128))
    spread = None
    for n in range(16):
        centered = branch[:, n * 128:(n + 1) * 128] - row_sums[...]
        spread = centered * centered if spread is None else spread + centered * centered
    var = jnp.sum(spread, axis=-1, keepdims=True) * (1.0 / 2048)
    inverse = jnp.broadcast_to(lax.rsqrt(var + EPSILON), (256, 128))
    for n in range(16):
        cols = slice(n * 128, (n + 1) * 128)
        normed[:, cols] = ((branch[:, cols] - row_sums[...]) * inverse * ng_ref[:, cols]).astype(BF16)
    w_last(7)()
    for kind in ("wd0", "wd1", "wd2", "wd3"):
        arrive(*[(kind, i) for i in range(8)])
    for lo, hi in ((0, 256), (256, 512), (512, 704)):
        gate = jnp.dot(normed[...], w_all[:, 0:32, lo:hi].reshape(2048, hi - lo), preferred_element_type=F32)
        upward = jnp.dot(normed[...], w_all[:, 32:64, lo:hi].reshape(2048, hi - lo), preferred_element_type=F32)
        hidden[:, lo:hi] = (gate / (1.0 + jnp.exp(-gate)) * upward).astype(BF16)
    for h in range(2):
        def down(n, carry):
            rows_of = pl.ds(pl.multiple_of((h * 4 + n) * 8, 8), 8)
            product = lax.dot_general(
                hidden[...], w_all[rows_of, 64:96, :].reshape(256, 704), (((1,), (1,)), ((), ())),
                preferred_element_type=F32,
            ).astype(BF16)
            cols = pl.ds(pl.multiple_of(n * 256, 256), 256)
            part[h, :, cols] = product
            return carry

        lax.fori_loop(0, 4, down, 0)
        start(("p", h, 2), ("p", h, 1), ("p", h, 3))
    own_rows = pl.ds(pl.multiple_of(x * 64, 64), 64)
    for h in range(2):
        for j in range(1, 4):
            arrive(("p", h, j))
        cols = slice(h * 1024, (h + 1) * 1024)
        mixer = part[h, own_rows, :].astype(F32)
        for j in range(1, 4):
            mixer += part_in[h, j].astype(F32)
        out_ref[:, cols] = (ALPHA * normed[own_rows, cols].astype(F32) + 0.5 * mixer).astype(BF16)
    for name in NAMES:
        describe(name).wait_send()


def on_device(
    stream, query_one, key_one, query_two, key_two, values, lambdas, head_gain, out_weight, norm_gain,
    gate_weight, up_weight, down_weight,
):
    whole = pl.BlockSpec(memory_space=pl.ANY)
    vmem = pl.BlockSpec(memory_space=pltpu.VMEM)
    return pl.pallas_call(
        kernel,
        out_shape=jax.ShapeDtypeStruct((64, 2048), BF16),
        in_specs=[whole] * 9 + [pl.BlockSpec(memory_space=pltpu.SMEM), vmem, vmem, whole],
        out_specs=vmem,
        scratch_shapes=[
            pltpu.VMEM((4, 256, 256), BF16),
            pltpu.VMEM((16, 256, 256), BF16),
            pltpu.VMEM((16, 256, 256), BF16),
            pltpu.VMEM((256, 256), BF16),
            pltpu.VMEM((16, 128, 256), F32),
            pltpu.VMEM((16, 8, 256), F32),
            pltpu.VMEM((16, 8, 256), F32),
            pltpu.VMEM((1024, 256), F32),
            pltpu.VMEM((1024, 256), F32),
            pltpu.VMEM((64, 96, 704), BF16),
            pltpu.VMEM((4, 64, 2048), BF16),
            pltpu.VMEM((1024, 2048), BF16),
            pltpu.VMEM((3, 512, 256), BF16),
            pltpu.VMEM((3, 8, 256), F32),
            pltpu.VMEM((3, 512, 256), BF16),
            pltpu.VMEM((3, 8, 256), F32),
            pltpu.VMEM((4, 256, 256), BF16),
            pltpu.VMEM((256, 2048), F32),
            pltpu.VMEM((256, 128), F32),
            pltpu.VMEM((256, 2048), BF16),
            pltpu.VMEM((256, 704), BF16),
            pltpu.VMEM((2, 256, 1024), BF16),
            pltpu.VMEM((2, 4, 64, 1024), BF16),
            pltpu.SemaphoreType.DMA((len(NAMES),)),
            pltpu.SemaphoreType.DMA((len(NAMES),)),
            pltpu.SemaphoreType.DMA((12,)),
        ],
        compiler_params=pltpu.CompilerParams(
            collective_id=0, has_side_effects=True, vmem_limit_bytes=60 * 2**20
        ),
    )(
        query_one, query_two, key_one, key_two, values, gate_weight, up_weight, jnp.transpose(down_weight), stream, lambdas, head_gain.reshape(1, 128), norm_gain.reshape(1, 2048),
        out_weight,
    )


def solution(mesh):
    return jax.shard_map(
        on_device,
        mesh=mesh,
        in_specs=(
            P(("sp", "tp"), None), P("sp", "tp"), P("sp", "tp"), P("sp", "tp"), P("sp", "tp"), P("sp", "tp"),
            P("tp"), P(), P(), P(), P("sp", "tp"), P("sp", "tp"), P("tp", "sp"),
        ),
        out_specs=P(("sp", "tp"), None),
        check_vma=False,
    )
```

time: 121 us -> 99.9 us (0.83)
  Pallas kernels: 119 us -> 98.1 us
    pallas_call x1, Pallas kernels: 119 us -> 98.1 us  [on_device(): pl.pallas_call(kernel, out_shape=jax.ShapeDtypeStruct((64, 2048), BF16),...]
where the time goes in v3:
time: 99.9 us; the launch traced here: 99.8 us
  Pallas kernels  98.1 us (98%)
  local copies, waits for them, and re-layouts  1.67 us (2%)
    pallas_call x1, Pallas kernels, on_device(): pl.pallas_call(kernel, out_shape=jax.ShapeDtypeStruct((64, 2048), BF16),...  98.1 us

profile of v3, /device:TPU:1, one launch (start us, length us, event | category | flops | bytes accessed | tf_op | source)
XLA Modules:
  0.0 99.8 jit_solution(7831039591304358993)
XLA Ops:
  0.0 98.1 %shard_map.127 = bf16[64,2048]{1,0:T(8,128)(2,1)} custom-call(bf16[256,128]{1,0:T(8,128)(2,1)} %q1_ref.1, bf16[256,128]{1,0:T(8,128)(2,1)} %q2_ref.1, bf16[256,128]{1,0:T(8,128)(2,1)} %k1_ref.1, bf16[256,128]{1,0:T(8,128)(2,1)} %k2_ref.1, bf16[256,256]{1,0:T(8,128)(2,1)} %v_ref.1, bf16[32,704]{1,0:T(8,128)(2,1)} %g_ref.1, bf16[32,704]{1,0:T(8,128)(2,1)} %u_ref.1, ...), custom_call_target="tpu_custom_call" | custom-call | tf_op jit(solution)/shard_map/pallas_call | solution.py:441
  98.1 1.7 %copy.15 = bf16[64,2048]{1,0:T(8,128)(2,1)} copy(bf16[64,2048]{1,0:T(8,128)(2,1)} %shard_map.127) | data formatting | bytes 524288

commit v4 on v3

--- a/solution.py
+++ b/solution.py
@@ -25,6 +25,8 @@
     names += [("wz", s) for s in range(1, 7)] + [("wz7a",), ("wz7b",)]
     for kind in ("wxl", "wxr", "wxa", "wxb", "wd0", "wd1", "wd2", "wd3"):
         names += [(kind, i) for i in range(8)]
+    names += [(kind,) for kind in ("dyl", "dyr", "dya", "dyb", "dz7a", "dz7b")]
+    names += [("dz", s) for s in range(1, 7)] + [("dd", i) for i in range(8)]
     names += [("s", j) for j in range(1, 4)]
     names += [("o", p) for p in range(1, 4)] + [("st", p) for p in range(1, 4)]
     names += [("a", j) for j in range(1, 4)]
@@ -39,7 +41,7 @@
 def kernel(
     q1_ref, q2_ref, k1_ref, k2_ref, v_ref, g_ref, u_ref, d_ref, s_ref, lam_ref, hg_ref, ng_ref, wo_ref,
     out_ref,
-    q_all, k_all, v_all, v_own, acc, m_st, l_st, sb0, sb1, w_all, s_all, wo_v,
+    q_all, k_all, v_all, v_own, acc, m_st, l_st, sb0, sb1, w_all, d_all, s_all, wo_v,
     o_out, st_out, o_in, st_in, att, branch, row_sums, normed, hidden, part, part_in,
     send_sems, recv_sems, local_sems,
 ):
@@ -91,22 +93,44 @@
             ref = w_all.at[block(dz=Z_OF_SLOT[s - 2] if s > 2 else 0)]
             return remote(name, ref, ref, at(dz=step))
         if kind == "wz7a":
-            ref = w_all.at[block(dz=-3), 0:48]
+            ref = w_all.at[block(dz=-3), 0:32]
             return remote(name, ref, ref, at(dz=1))
         if kind == "wz7b":
-            ref = w_all.at[block(dz=3), 48:96]
+            ref = w_all.at[block(dz=3), 32:64]
             return remote(name, ref, ref, at(dz=-1))
         if kind in ("wxl", "wxr"):
             ref = w_all.at[block(dz=Z_OF_SLOT[name[1]])]
             return remote(name, ref, ref, at(dy=1 if kind == "wxl" else -1))
         if kind == "wxa":
-            ref = w_all.at[block(dz=Z_OF_SLOT[name[1]], dy=-1), 0:48]
+            ref = w_all.at[block(dz=Z_OF_SLOT[name[1]], dy=-1), 0:32]
             return remote(name, ref, ref, at(dy=1))
         if kind == "wxb":
-            ref = w_all.at[block(dz=Z_OF_SLOT[name[1]], dy=1), 48:96]
+            ref = w_all.at[block(dz=Z_OF_SLOT[name[1]], dy=1), 32:64]
             return remote(name, ref, ref, at(dy=-1))
         if kind[:2] == "wd":
             ref = w_all.at[block(dz=Z_OF_SLOT[name[1]], dy=(0, -1, 1, 2)[int(kind[2])])]
+            return remote(name, ref, ref, at(dc=1))
+        if kind in ("dyl", "dyr"):
+            ref = d_all.at[z, c, y]
+            return remote(name, ref, ref, at(dy=1 if kind == "dyl" else -1))
+        if kind == "dya":
+            ref = d_all.at[z, c, mod(y - 1, 4), 0:16]
+            return remote(name, ref, ref, at(dy=1))
+        if kind == "dyb":
+            ref = d_all.at[z, c, mod(y + 1, 4), 16:32]
+            return remote(name, ref, ref, at(dy=-1))
+        if kind == "dz":
+            s = name[1]
+            ref = d_all.at[mod(z + (Z_OF_SLOT[s - 2] if s > 2 else 0), 8), c]
+            return remote(name, ref, ref, at(dz=1 if s in (1, 3, 5) else -1))
+        if kind == "dz7a":
+            ref = d_all.at[mod(z - 3, 8), c, 0:2]
+            return remote(name, ref, ref, at(dz=1))
+        if kind == "dz7b":
+            ref = d_all.at[mod(z + 3, 8), c, 2:4]
+            return remote(name, ref, ref, at(dz=-1))
+        if kind == "dd":
+            ref = d_all.at[mod(z + Z_OF_SLOT[name[1]], 8), c]
             return remote(name, ref, ref, at(dc=1))
         if kind == "s":
             return remote(name, s_all.at[x], s_all.at[x], at(dx=name[1]))
@@ -142,7 +166,7 @@
         for i, (src, dst) in enumerate((
             (v_ref, v_own), (q1_ref, q_all.at[0, :, 0:128]), (q2_ref, q_all.at[0, :, 128:256]),
             (k1_ref, k_all.at[0, :, 0:128]), (k2_ref, k_all.at[0, :, 128:256]),
-            (g_ref, w_all.at[sp, 0:32]), (u_ref, w_all.at[sp, 32:64]), (d_ref, w_all.at[sp, 64:96]), (s_ref, s_all.at[x]),
+            (g_ref, w_all.at[sp, 0:32]), (u_ref, w_all.at[sp, 32:64]), (d_ref, d_all.at[z, c, y]), (s_ref, s_all.at[x]),
         ))
     ]
     for take in takes:
@@ -223,36 +247,57 @@
             start(("o", p), ("st", p))
         return act
 
+    def d_first():
+        start(("dyl",), ("dyr",))
+
+    def d_on():
+        arrive(("dyl",), ("dyr",))
+        start(("dya",), ("dyb",))
+
+    def d_last():
+        arrive(("dya",), ("dyb",))
+        start(("dd", 0))
+
+    def d_ring(s):
+        def act():
+            arrive(("dz", s), ("dz", s + 1))
+            if s < 5:
+                start(("dz", s + 2), ("dz", s + 3))
+            else:
+                start(("dz7a",), ("dz7b",))
+            start(("dd", s), ("dd", s + 1))
+        return act
+
     phases = (
         (0, 2, (
             (got(("kd", 0), ("vd", 0)),),
-            (got(("q", 2)), on("k", 1), lambda: start(("wz", 1), ("wz", 2)), w_across(0)),
+            (got(("q", 2)), on("k", 1), lambda: start(("wz", 1), ("wz", 2)), w_across(0), d_first),
             (got(("q", 3)), on("v", 1)),
             (got(("kd", 1), ("kd", 2)),),
         )),
         (2, 4, (
             (got(("vd", 1), ("vd", 2)), lambda: start(("s", 1), ("s", 3), ("s", 2))),
-            (on("k", 3), w_on(0)),
+            (on("k", 3), w_on(0), d_on),
             (w_ring(1), w_next(1)),
             (on("v", 3), got(("kd", 3), ("kd", 4))),
         )),
         (6, 4, (
             (got(("vd", 3), ("vd", 4)),),
-            (w_last(0),),
+            (w_last(0), d_last),
             (on("k", 5),),
             (got(("kd", 5), ("kd", 6)), w_on(1)),
         )),
         (10, 4, (
-            (on("v", 5), w_ring(3), got(("vd", 5), ("vd", 6))),
+            (on("v", 5), w_ring(3), w_next(3), lambda: start(("dz", 1), ("dz", 2)), got(("vd", 5), ("vd", 6))),
             (w_on(2),),
-            (w_last(1), w_next(3)),
+            (w_last(1), w_on(3)),
             (ring_end, got(("kd", 7))),
         )),
         (14, 2, (
-            (got(("vd", 7)), w_on(3)),
-            (finalize(3), w_last(2)),
+            (got(("vd", 7)),),
+            (finalize(3), w_on(4), w_last(2)),
             (finalize(2),),
-            (finalize(1), w_on(4)),
+            (finalize(1), w_ring(5), w_next(5)),
         )),
     )
 
@@ -336,9 +381,10 @@
             peak = visit(3, first, count, peak, opening, ahead[0], ahead[1])
 
     w_last(3)()
-    w_ring(5)()
-    w_next(5)()
+    d_ring(1)()
     arrive(("o", 3), ("st", 3))
+    w_ring_end()
+    w_across(7)()
     arrive(("o", 2), ("st", 2))
     arrive(("o", 1), ("st", 1))
     for h in range(2):
@@ -362,11 +408,11 @@
         att[x, :, h * 128:(h + 1) * 128] = (scaled * hg_ref[...] * 0.8).astype(BF16)
     exchange = [("a", 2), ("a", 1), ("a", 3)]
     start(*exchange)
-    w_ring_end()
-    w_across(7)()
     w_last(4)()
     w_on(5)()
     w_on(6)()
+    d_ring(3)()
+    w_on(7)()
     wo_copy.wait()
     arrive(*exchange)
 
@@ -387,7 +433,7 @@
     lax.fori_loop(0, 4, project, 0)
     w_last(5)()
     w_last(6)()
-    w_on(7)()
+    d_ring(5)()
     mean = jnp.sum(row_sums[...], axis=-1, keepdims=True) * (1.0 / 2048)
     row_sums[...] = jnp.broadcast_to(mean, (256, 128))
     spread = None
@@ -400,17 +446,20 @@
         cols = slice(n * 128, (n + 1) * 128)
         normed[:, cols] = ((branch[:, cols] - row_sums[...]) * inverse * ng_ref[:, cols]).astype(BF16)
     w_last(7)()
+    arrive(("dz7a",), ("dz7b",))
+    start(("dd", 7))
     for kind in ("wd0", "wd1", "wd2", "wd3"):
         arrive(*[(kind, i) for i in range(8)])
     for lo, hi in ((0, 256), (256, 512), (512, 704)):
         gate = jnp.dot(normed[...], w_all[:, 0:32, lo:hi].reshape(2048, hi - lo), preferred_element_type=F32)
         upward = jnp.dot(normed[...], w_all[:, 32:64, lo:hi].reshape(2048, hi - lo), preferred_element_type=F32)
         hidden[:, lo:hi] = (gate / (1.0 + jnp.exp(-gate)) * upward).astype(BF16)
+    arrive(*[("dd", i) for i in range(8)])
     for h in range(2):
         def down(n, carry):
-            rows_of = pl.ds(pl.multiple_of((h * 4 + n) * 8, 8), 8)
+            columns = jnp.concatenate([d_all[h * 4 + n, i % 2, i // 2] for i in range(8)], axis=0)
             product = lax.dot_general(
-                hidden[...], w_all[rows_of, 64:96, :].reshape(256, 704), (((1,), (1,)), ((), ())),
+                hidden[...], columns, (((1,), (1,)), ((), ())),
                 preferred_element_type=F32,
             ).astype(BF16)
             cols = pl.ds(pl.multiple_of(n * 256, 256), 256)
@@ -453,7 +502,8 @@
             pltpu.VMEM((16, 8, 256), F32),
             pltpu.VMEM((1024, 256), F32),
             pltpu.VMEM((1024, 256), F32),
-            pltpu.VMEM((64, 96, 704), BF16),
+            pltpu.VMEM((64, 64, 704), BF16),
+            pltpu.VMEM((8, 2, 4, 32, 704), BF16),
             pltpu.VMEM((4, 64, 2048), BF16),
             pltpu.VMEM((1024, 2048), BF16),
             pltpu.VMEM((3, 512, 256), BF16),

time: 99.9 us -> 95.2 us (0.953)
  Pallas kernels: 98.1 us -> 93.4 us
    pallas_call x1, Pallas kernels: 98.1 us -> 93.4 us  [on_device(): pl.pallas_call(kernel, out_shape=jax.ShapeDtypeStruct((64, 2048), BF16),...]
where the time goes in v4:
time: 95.2 us; the launch traced here: 95.1 us
  Pallas kernels  93.4 us (98%)
  local copies, waits for them, and re-layouts  1.67 us (2%)
    pallas_call x1, Pallas kernels, on_device(): pl.pallas_call(kernel, out_shape=jax.ShapeDtypeStruct((64, 2048), BF16),...  93.4 us

profile of v4, /device:TPU:1, one launch (start us, length us, event | category | flops | bytes accessed | tf_op | source)
XLA Modules:
  0.0 95.1 jit_solution(17434234606184425740)
XLA Ops:
  0.0 93.4 %shard_map.127 = bf16[64,2048]{1,0:T(8,128)(2,1)} custom-call(bf16[256,128]{1,0:T(8,128)(2,1)} %q1_ref.1, bf16[256,128]{1,0:T(8,128)(2,1)} %q2_ref.1, bf16[256,128]{1,0:T(8,128)(2,1)} %k1_ref.1, bf16[256,128]{1,0:T(8,128)(2,1)} %k2_ref.1, bf16[256,256]{1,0:T(8,128)(2,1)} %v_ref.1, bf16[32,704]{1,0:T(8,128)(2,1)} %g_ref.1, bf16[32,704]{1,0:T(8,128)(2,1)} %u_ref.1, ...), custom_call_target="tpu_custom_call" | custom-call | tf_op jit(solution)/shard_map/pallas_call | solution.py:490
  93.4 1.7 %copy.15 = bf16[64,2048]{1,0:T(8,128)(2,1)} copy(bf16[64,2048]{1,0:T(8,128)(2,1)} %shard_map.127) | data formatting | bytes 524288

commit v5 on v4

--- a/solution.py
+++ b/solution.py
@@ -30,7 +30,7 @@
     names += [("s", j) for j in range(1, 4)]
     names += [("o", p) for p in range(1, 4)] + [("st", p) for p in range(1, 4)]
     names += [("a", j) for j in range(1, 4)]
-    names += [("p", h, j) for h in range(2) for j in range(1, 4)]
+    names += [(kind, h) for kind in ("fa", "fb", "u1", "u3", "m1", "m3") for h in range(2)]
     return names
 
 
@@ -42,7 +42,7 @@
     q1_ref, q2_ref, k1_ref, k2_ref, v_ref, g_ref, u_ref, d_ref, s_ref, lam_ref, hg_ref, ng_ref, wo_ref,
     out_ref,
     q_all, k_all, v_all, v_own, acc, m_st, l_st, sb0, sb1, w_all, d_all, s_all, wo_v,
-    o_out, st_out, o_in, st_in, att, branch, row_sums, normed, hidden, part, part_in,
+    o_out, st_out, o_in, st_in, att, branch, row_sums, normed, hidden, part, part_in, far_in, merged_out,
     send_sems, recv_sems, local_sems,
 ):
     sp = lax.axis_index("sp")
@@ -62,6 +62,9 @@
 
     def block(dz=0, dy=0):
         return mod(z + dz, 8) * 8 + mod(y + dy, 4) * 2 + c
+
+    def partial_rows(j, offset):
+        return pl.ds(pl.multiple_of(mod(x - j, 4) * 64 + offset, 32), 32)
 
     def remote(name, src, dst, target):
         i = INDEX[name]
@@ -142,10 +145,19 @@
             return remote(name, st_out.at[p - 1], st_in.at[p - 1], at(dy=-REL[p]))
         if kind == "a":
             return remote(name, att.at[x], att.at[x], at(dx=name[1]))
-        if kind == "p":
-            h, j = name[1:]
-            rows = pl.multiple_of(mod(x - j, 4) * 64, 64)
-            return remote(name, part.at[h, pl.ds(rows, 64)], part_in.at[h, j], at(dx=-j))
+        h = name[1]
+        if kind == "fa":
+            return remote(name, part.at[h, partial_rows(2, 0)], far_in.at[h, 0], at(dx=-1))
+        if kind == "fb":
+            return remote(name, part.at[h, partial_rows(2, 32)], far_in.at[h, 1], at(dx=1))
+        if kind == "u1":
+            return remote(name, part.at[h, partial_rows(1, 32)], part_in.at[h, 0, 32:64], at(dx=-1))
+        if kind == "u3":
+            return remote(name, part.at[h, partial_rows(3, 0)], part_in.at[h, 1, 0:32], at(dx=1))
+        if kind == "m1":
+            return remote(name, merged_out.at[h, 0], part_in.at[h, 0, 0:32], at(dx=-1))
+        if kind == "m3":
+            return remote(name, merged_out.at[h, 1], part_in.at[h, 1, 32:64], at(dx=1))
         raise KeyError(kind)
 
     def start(*names):
@@ -297,7 +309,7 @@
             (got(("vd", 7)),),
             (finalize(3), w_on(4), w_last(2)),
             (finalize(2),),
-            (finalize(1), w_ring(5), w_next(5)),
+            (finalize(1), got(("wz", 5), ("wz", 6)), w_next(5)),
         )),
     )
 
@@ -383,10 +395,13 @@
     w_last(3)()
     d_ring(1)()
     arrive(("o", 3), ("st", 3))
+    w_across(5)()
+    w_across(6)()
     w_ring_end()
-    w_across(7)()
+    d_ring(3)()
     arrive(("o", 2), ("st", 2))
     arrive(("o", 1), ("st", 1))
+    w_across(7)()
     for h in range(2):
         maps = []
         for m in range(2):
@@ -409,9 +424,9 @@
     exchange = [("a", 2), ("a", 1), ("a", 3)]
     start(*exchange)
     w_last(4)()
+    d_ring(5)()
     w_on(5)()
     w_on(6)()
-    d_ring(3)()
     w_on(7)()
     wo_copy.wait()
     arrive(*exchange)
@@ -433,7 +448,8 @@
     lax.fori_loop(0, 4, project, 0)
     w_last(5)()
     w_last(6)()
-    d_ring(5)()
+    arrive(("dz7a",), ("dz7b",))
+    start(("dd", 7))
     mean = jnp.sum(row_sums[...], axis=-1, keepdims=True) * (1.0 / 2048)
     row_sums[...] = jnp.broadcast_to(mean, (256, 128))
     spread = None
@@ -446,8 +462,6 @@
         cols = slice(n * 128, (n + 1) * 128)
         normed[:, cols] = ((branch[:, cols] - row_sums[...]) * inverse * ng_ref[:, cols]).astype(BF16)
     w_last(7)()
-    arrive(("dz7a",), ("dz7b",))
-    start(("dd", 7))
     for kind in ("wd0", "wd1", "wd2", "wd3"):
         arrive(*[(kind, i) for i in range(8)])
     for lo, hi in ((0, 256), (256, 512), (512, 704)):
@@ -467,15 +481,20 @@
             return carry
 
         lax.fori_loop(0, 4, down, 0)
-        start(("p", h, 2), ("p", h, 1), ("p", h, 3))
+        start(("fa", h), ("fb", h), ("u1", h), ("u3", h))
+    for h in range(2):
+        arrive(("fa", h), ("fb", h))
+        for side, (j, offset) in enumerate(((1, 0), (3, 32))):
+            own = part[h, partial_rows(j, offset), :].astype(F32)
+            merged_out[h, side] = (own + far_in[h, side].astype(F32)).astype(BF16)
+        start(("m1", h), ("m3", h))
     own_rows = pl.ds(pl.multiple_of(x * 64, 64), 64)
     for h in range(2):
-        for j in range(1, 4):
-            arrive(("p", h, j))
+        arrive(("u1", h), ("u3", h), ("m1", h), ("m3", h))
         cols = slice(h * 1024, (h + 1) * 1024)
         mixer = part[h, own_rows, :].astype(F32)
-        for j in range(1, 4):
-            mixer += part_in[h, j].astype(F32)
+        for side in range(2):
+            mixer += part_in[h, side].astype(F32)
         out_ref[:, cols] = (ALPHA * normed[own_rows, cols].astype(F32) + 0.5 * mixer).astype(BF16)
     for name in NAMES:
         describe(name).wait_send()
@@ -516,7 +535,9 @@
             pltpu.VMEM((256, 2048), BF16),
             pltpu.VMEM((256, 704), BF16),
             pltpu.VMEM((2, 256, 1024), BF16),
-            pltpu.VMEM((2, 4, 64, 1024), BF16),
+            pltpu.VMEM((2, 2, 64, 1024), BF16),
+            pltpu.VMEM((2, 2, 32, 1024), BF16),
+            pltpu.VMEM((2, 2, 32, 1024), BF16),
             pltpu.SemaphoreType.DMA((len(NAMES),)),
             pltpu.SemaphoreType.DMA((len(NAMES),)),
             pltpu.SemaphoreType.DMA((12,)),

time: 95.2 us -> 90 us (0.945)
  Pallas kernels: 93.4 us -> 88.1 us
    pallas_call x1, Pallas kernels: 93.4 us -> 88.1 us  [on_device(): pl.pallas_call(kernel, out_shape=jax.ShapeDtypeStruct((64, 2048), BF16),...]
where the time goes in v5:
time: 90 us; the launch traced here: 89.8 us
  Pallas kernels  88.1 us (98%)
  local copies, waits for them, and re-layouts  1.67 us (2%)
    pallas_call x1, Pallas kernels, on_device(): pl.pallas_call(kernel, out_shape=jax.ShapeDtypeStruct((64, 2048), BF16),...  88.1 us

profile of v5, /device:TPU:1, one launch (start us, length us, event | category | flops | bytes accessed | tf_op | source)
XLA Modules:
  0.0 89.8 jit_solution(13770182578038627180)
XLA Ops:
  0.0 88.1 %shard_map.127 = bf16[64,2048]{1,0:T(8,128)(2,1)} custom-call(bf16[256,128]{1,0:T(8,128)(2,1)} %q1_ref.1, bf16[256,128]{1,0:T(8,128)(2,1)} %q2_ref.1, bf16[256,128]{1,0:T(8,128)(2,1)} %k1_ref.1, bf16[256,128]{1,0:T(8,128)(2,1)} %k2_ref.1, bf16[256,256]{1,0:T(8,128)(2,1)} %v_ref.1, bf16[32,704]{1,0:T(8,128)(2,1)} %g_ref.1, bf16[32,704]{1,0:T(8,128)(2,1)} %u_ref.1, ...), custom_call_target="tpu_custom_call" | custom-call | tf_op jit(solution)/shard_map/pallas_call | solution.py:509
  88.1 1.7 %copy.15 = bf16[64,2048]{1,0:T(8,128)(2,1)} copy(bf16[64,2048]{1,0:T(8,128)(2,1)} %shard_map.127) | data formatting | bytes 524288

commit v6 on v5

--- a/solution.py
+++ b/solution.py
@@ -185,9 +185,6 @@
         take.start()
     wo_copy = pltpu.make_async_copy(wo_ref, wo_v, local_sems.at[0])
     wo_copy.start()
-    m_st[...] = jnp.full_like(m_st, -1e30)
-    l_st[...] = jnp.zeros_like(l_st)
-    acc[...] = jnp.zeros_like(acc)
     takes[0].wait()
     v_all[0] = jnp.transpose(v_own[...])
     for take in takes[1:]:
@@ -195,6 +192,9 @@
     pl.semaphore_wait(barrier, len(partners))
 
     start(("q", 1), ("q", 2), ("kd", 0), ("k", 1), ("k", 2), ("vd", 0), ("v", 1), ("v", 2), ("q", 3))
+    m_st[...] = jnp.full_like(m_st, -1e30)
+    l_st[...] = jnp.zeros_like(l_st)
+    acc[...] = jnp.zeros_like(acc)
 
     def w_across(i):
         def act():
@@ -297,16 +297,16 @@
             (got(("vd", 3), ("vd", 4)),),
             (w_last(0), d_last),
             (on("k", 5),),
-            (got(("kd", 5), ("kd", 6)), w_on(1)),
+            (got(("kd", 5), ("kd", 6)), w_on(1), on("v", 5)),
         )),
         (10, 4, (
-            (on("v", 5), w_ring(3), w_next(3), lambda: start(("dz", 1), ("dz", 2)), got(("vd", 5), ("vd", 6))),
+            (w_ring(3), w_next(3), lambda: start(("dz", 1), ("dz", 2)), got(("vd", 5), ("vd", 6))),
             (w_on(2),),
-            (w_last(1), w_on(3)),
+            (w_last(1),),
             (ring_end, got(("kd", 7))),
         )),
         (14, 2, (
-            (got(("vd", 7)),),
+            (got(("vd", 7)), w_on(3)),
             (finalize(3), w_on(4), w_last(2)),
             (finalize(2),),
             (finalize(1), got(("wz", 5), ("wz", 6)), w_next(5)),

time: 90 us -> 90.1 us (level)
  no operation moved by 1% of the time
where the time goes in v6:
time: 90.1 us; the launch traced here: 90 us
  Pallas kernels  88.3 us (98%)
  local copies, waits for them, and re-layouts  1.67 us (2%)
    pallas_call x1, Pallas kernels, on_device(): pl.pallas_call(kernel, out_shape=jax.ShapeDtypeStruct((64, 2048), BF16),...  88.3 us

profile of v6, /device:TPU:1, one launch (start us, length us, event | category | flops | bytes accessed | tf_op | source)
XLA Modules:
  0.0 90.0 jit_solution(14177134849941774457)
XLA Ops:
  0.0 88.3 %shard_map.127 = bf16[64,2048]{1,0:T(8,128)(2,1)} custom-call(bf16[256,128]{1,0:T(8,128)(2,1)} %q1_ref.1, bf16[256,128]{1,0:T(8,128)(2,1)} %q2_ref.1, bf16[256,128]{1,0:T(8,128)(2,1)} %k1_ref.1, bf16[256,128]{1,0:T(8,128)(2,1)} %k2_ref.1, bf16[256,256]{1,0:T(8,128)(2,1)} %v_ref.1, bf16[32,704]{1,0:T(8,128)(2,1)} %g_ref.1, bf16[32,704]{1,0:T(8,128)(2,1)} %u_ref.1, ...), custom_call_target="tpu_custom_call" | custom-call | tf_op jit(solution)/shard_map/pallas_call | solution.py:509
  88.3 1.7 %copy.15 = bf16[64,2048]{1,0:T(8,128)(2,1)} copy(bf16[64,2048]{1,0:T(8,128)(2,1)} %shard_map.127) | data formatting | bytes 524288

commit v7 on v6

--- a/solution.py
+++ b/solution.py
@@ -445,7 +445,7 @@
         row_sums[...] += sum(mixed[:, i * 128:(i + 1) * 128] for i in range(4))
         return carry
 
-    lax.fori_loop(0, 4, project, 0)
+    lax.fori_loop(0, 4, project, 0, unroll=True)
     w_last(5)()
     w_last(6)()
     arrive(("dz7a",), ("dz7b",))
@@ -480,7 +480,7 @@
             part[h, :, cols] = product
             return carry
 
-        lax.fori_loop(0, 4, down, 0)
+        lax.fori_loop(0, 4, down, 0, unroll=True)
         start(("fa", h), ("fb", h), ("u1", h), ("u3", h))
     for h in range(2):
         arrive(("fa", h), ("fb", h))

time: 90.1 us -> 88.7 us (0.984)
  Pallas kernels: 88.3 us -> 86.9 us
    pallas_call x1, Pallas kernels: 88.3 us -> 86.9 us  [on_device(): pl.pallas_call(kernel, out_shape=jax.ShapeDtypeStruct((64, 2048), BF16),...]
where the time goes in v7:
time: 88.7 us; the launch traced here: 88.5 us
  Pallas kernels  86.9 us (98%)
  local copies, waits for them, and re-layouts  1.67 us (2%)
    pallas_call x1, Pallas kernels, on_device(): pl.pallas_call(kernel, out_shape=jax.ShapeDtypeStruct((64, 2048), BF16),...  86.9 us

profile of v7, /device:TPU:1, one launch (start us, length us, event | category | flops | bytes accessed | tf_op | source)
XLA Modules:
  0.0 88.5 jit_solution(16626049348174925315)
XLA Ops:
  0.0 86.9 %shard_map.127 = bf16[64,2048]{1,0:T(8,128)(2,1)} custom-call(bf16[256,128]{1,0:T(8,128)(2,1)} %q1_ref.1, bf16[256,128]{1,0:T(8,128)(2,1)} %q2_ref.1, bf16[256,128]{1,0:T(8,128)(2,1)} %k1_ref.1, bf16[256,128]{1,0:T(8,128)(2,1)} %k2_ref.1, bf16[256,256]{1,0:T(8,128)(2,1)} %v_ref.1, bf16[32,704]{1,0:T(8,128)(2,1)} %g_ref.1, bf16[32,704]{1,0:T(8,128)(2,1)} %u_ref.1, ...), custom_call_target="tpu_custom_call" | custom-call | tf_op jit(solution)/shard_map/pallas_call | solution.py:509
  86.9 1.7 %copy.15 = bf16[64,2048]{1,0:T(8,128)(2,1)} copy(bf16[64,2048]{1,0:T(8,128)(2,1)} %shard_map.127) | data formatting | bytes 524288
